TPU v7x, 512 devices: a whole 4x8x8 slice. The times are simulated.
512 devices in a mesh: sp: 32 (over z, x), tp: 16 (over y, core).
Axes of the slice: x: 4, y: 8, z: 8, core: 2. Of those that a mesh axis runs over, the one named last changes fastest.
Arguments:
- residual_in: bfloat16 [4096, 2048], P('sp', 'tp'), may hold values from -8 to 8
- query_alpha: bfloat16 [4096, 2048], P('sp', 'tp'), may hold values from -8 to 8
- pairs_alpha: bfloat16 [4096, 16, 128], P('sp', 'tp'), may hold values from -8 to 8
- offset_alpha: float32 [4096, 32], P('sp', 'tp'), may hold values from -18 to -1
- gain_alpha: float32 [2048], P('tp'), may hold values from 0.1 to 1.9
- query_beta: bfloat16 [4096, 2048], P('sp', 'tp'), may hold values from -8 to 8
- pairs_beta: bfloat16 [4096, 16, 256], P('sp', 'tp'), may hold values from -8 to 8
- offset_beta: float32 [4096, 16], P('sp', 'tp'), may hold values from -18 to -1
- gain_beta: float32 [2048], P('tp'), may hold values from 0.1 to 1.9
- project_alpha: bfloat16 [2048, 2048], P('tp'), may hold values from -0.09375 to 0.09375
- project_beta: bfloat16 [2048, 2048], P('tp'), may hold values from -0.09375 to 0.09375
- gain_settle: float32 [2048], P('tp'), may hold values from 0 to 4
- bias_settle: float32 [2048], P('tp'), may hold values from -2.5 to 2.5
- expert_ids: int32 [4096, 2], P('sp'), may hold values from 0 to 31, as said below
- route_weight: float32 [4096, 2], P('sp'), may hold values from 0.1 to 0.9
- expert_gate: bfloat16 [32, 2048, 4096], P('sp', None, 'tp'), may hold values from -0.125 to 0.125
- expert_up: bfloat16 [32, 2048, 4096], P('sp', None, 'tp'), may hold values from -0.125 to 0.125
- expert_down: bfloat16 [32, 4096, 2048], P('sp', 'tp'), may hold values from -0.1875 to 0.1875
- gain_final: float32 [2048], P('tp'), may hold values from 0.1 to 1.9
- bias_final: float32 [2048], P('tp'), may hold values from -2.5 to 2.5
Outputs:
- layer_out: bfloat16 [4096, 2048], P('sp', 'tp')
Inputs may be any that keep to these rules, and one draw needn't show every extreme that they name: `expert_ids`: the two numbers of a row differ and lie in one group of 8 consecutive experts. Among the rows of one device, no expert is named more than 12 times, and every expert of one group, the same group for all devices, is named exactly 12 times.
All inputs are finite; a program needn't handle non-finite values.
Results may differ from a plain program's by a relative error of at most 0.018.
Values may be sent and summed in bfloat16 or wider, within the bound.
A program may use at most 64 MiB of HBM per device.

v0:
```python
import jax
import jax.numpy as jnp
from jax import lax
from jax.sharding import PartitionSpec as P

depth_scale = 2.0**0.5
norm_eps = 1e-05


def joined_along(parts, dim):
    dims = list(parts.shape[1:])
    dims[dim] *= parts.shape[0]
    return jnp.moveaxis(parts, 0, dim).reshape(dims)


def gather_packed(arrays, axis, dims):
    flat = jnp.concatenate([a.reshape(-1) for a in arrays])
    lines, at, finished = (lax.all_gather(flat, axis), 0, [])
    for a, dim in zip(arrays, dims):
        parts = lines[:, at : at + a.size].reshape(-1, *a.shape)
        finished.append(joined_along(parts, dim))
        at += a.size
    return tuple(finished)


def sent_together(arrays, axis, dim, along):
    ends, at = ([], 0)
    for a in arrays[:-1]:
        at += a.shape[along]
        ends.append(at)
    both = jnp.concatenate(arrays, axis=along)
    return tuple(jnp.split(lax.all_gather(both, axis, axis=dim, tiled=True), ends, axis=along))


def sent_to_all(shard, axis):
    copies = jnp.broadcast_to(shard, (lax.axis_size(axis), *shard.shape))
    return lax.all_to_all(copies, axis, split_axis=0, concat_axis=0, tiled=True)


def over_copies(shard, axis):
    return sent_to_all(shard, axis).sum(axis=0)


def together(arrays, axis):
    flat, at, finished = (jnp.concatenate([a.reshape(-1) for a in arrays]), 0, [])
    running = over_copies(flat, axis)
    for a in arrays:
        finished.append(running[at : at + a.size].reshape(a.shape))
        at += a.size
    return tuple(finished)


def split_up(shard, dim, length):
    before, after = (shard.shape[:dim], shard.shape[dim + 1 :])
    return jnp.moveaxis(shard.reshape(*before, length, -1, *after), dim, 0)


def summed_on_arrival(shard, axis, dim):
    length = lax.axis_size(axis)
    parts = lax.all_to_all(split_up(shard, dim, length), axis, 0, 0, tiled=True)
    return jnp.sum(parts.astype(jnp.float32), axis=0)


def break_block(acc, remain, queries, pairs, offsets, key_first, query_first):
    width = queries.shape[3]
    keys = pairs[:, :, :width]
    values = pairs[:, :, width:]
    length = offsets.shape[0]
    kv_heads = queries.shape[1]
    share = queries.shape[2]
    scores = jnp.einsum(
        "qhrd,khd->hrqk", queries, keys, preferred_element_type=jnp.float32
    ) * width ** (-0.5)
    scores = (
        scores + jnp.transpose(offsets.reshape(length, kv_heads, share), (1, 2, 0))[:, :, None, :]
    )
    query_pos = query_first + jnp.arange(queries.shape[0], dtype=jnp.int32)
    key_pos = key_first + jnp.arange(length, dtype=jnp.int32)
    valid = key_pos[None, :] < query_pos[:, None]
    soft = jnp.where(valid, jax.nn.softplus(scores), 0.0)
    later = lax.cumsum(soft, axis=3, reverse=True) - soft
    weights = jnp.where(
        valid, jnp.exp(jax.nn.log_sigmoid(scores) - later + remain[..., None]), 0.0
    ).astype(jnp.bfloat16)
    acc = acc + jnp.einsum("hrqk,khd->qhrd", weights, values, preferred_element_type=jnp.float32)
    return (acc, remain - jnp.sum(soft, axis=3))


def finish_norm(total, sums, gain, bias, columns):
    mean = sums[0] / columns
    var = sums[1] / columns - mean * mean
    return ((total - mean[:, None]) * lax.rsqrt(var + norm_eps)[:, None] * gain + bias).astype(
        jnp.bfloat16
    )


def body(
    residual_in,
    query_alpha,
    pairs_alpha,
    offset_alpha,
    gain_alpha,
    query_beta,
    pairs_beta,
    offset_beta,
    gain_beta,
    project_alpha,
    project_beta,
    gain_settle,
    bias_settle,
    expert_ids,
    route_weight,
    expert_gate,
    expert_up,
    expert_down,
    gain_final,
    bias_final,
):
    rows = residual_in.shape[0]
    mine = lax.axis_index("sp")
    count = lax.axis_size("sp")
    heads_tp = lax.axis_size("tp")
    width_alpha = pairs_alpha.shape[2] // 2
    width_beta = pairs_beta.shape[2] // 2
    grouped_alpha = query_alpha.reshape(rows, pairs_alpha.shape[1], -1, width_alpha)
    grouped_beta = query_beta.reshape(rows, pairs_beta.shape[1], -1, width_beta)
    query_first = mine * rows
    initial = (
        jnp.zeros(grouped_alpha.shape, jnp.float32),
        jnp.zeros(grouped_beta.shape, jnp.float32),
        jnp.zeros((grouped_alpha.shape[1], grouped_alpha.shape[2], rows), jnp.float32),
        jnp.zeros((grouped_beta.shape[1], grouped_beta.shape[2], rows), jnp.float32),
    )

    def visit(state, pairs, offsets, key_first):
        acc_alpha, acc_beta, rest_alpha, rest_beta = state
        acc_alpha, rest_alpha = break_block(
            acc_alpha, rest_alpha, grouped_alpha, pairs[0], offsets[0], key_first, query_first
        )
        acc_beta, rest_beta = break_block(
            acc_beta, rest_beta, grouped_beta, pairs[1], offsets[1], key_first, query_first
        )
        return (acc_alpha, acc_beta, rest_alpha, rest_beta)

    def maybe_visit(state, turn, pairs, offsets):
        return lax.cond(
            turn <= mine,
            lambda kept: visit(kept, pairs, offsets, (mine - turn) * rows),
            lambda kept: kept,
            state,
        )

    pairs_all = gather_packed((pairs_alpha, pairs_beta), "sp", (0, 0))
    offsets_all = sent_together((offset_alpha, offset_beta), "sp", 0, 1)

    def turn_all(turn, state):
        first_row = (mine - turn) * rows
        pairs = (
            lax.dynamic_slice_in_dim(pairs_all[0], first_row, rows, 0),
            lax.dynamic_slice_in_dim(pairs_all[1], first_row, rows, 0),
        )
        offsets = (
            lax.dynamic_slice_in_dim(offsets_all[0], first_row, rows, 0),
            lax.dynamic_slice_in_dim(offsets_all[1], first_row, rows, 0),
        )
        return maybe_visit(state, turn, pairs, offsets)

    state = lax.fori_loop(0, count, turn_all, initial)
    attend_alpha = state[0].reshape(rows, -1)
    attend_beta = state[1].reshape(rows, -1)
    squares = together(
        (jnp.sum(attend_alpha * attend_alpha, axis=1), jnp.sum(attend_beta * attend_beta, axis=1)),
        "tp",
    )
    scale_alpha = lax.rsqrt(squares[0] / (attend_alpha.shape[1] * heads_tp) + norm_eps)
    scale_beta = lax.rsqrt(squares[1] / (attend_beta.shape[1] * heads_tp) + norm_eps)
    normed_alpha = (attend_alpha * scale_alpha[:, None] * gain_alpha).astype(jnp.bfloat16)
    normed_beta = (attend_beta * scale_beta[:, None] * gain_beta).astype(jnp.bfloat16)
    term = jnp.dot(normed_alpha, project_alpha, preferred_element_type=jnp.float32) + jnp.dot(
        normed_beta, project_beta, preferred_element_type=jnp.float32
    )
    mixed = summed_on_arrival(term.astype(jnp.bfloat16), "tp", 1).astype(jnp.bfloat16)
    columns = residual_in.shape[1] * heads_tp
    first = depth_scale * residual_in.astype(jnp.float32) + mixed.astype(jnp.float32)
    sums_one = together((jnp.sum(first, axis=1), jnp.sum(first * first, axis=1)), "tp")
    settled = finish_norm(first, sums_one, gain_settle, bias_settle, columns)
    cap = 3 * rows // count
    flat_ids = expert_ids.reshape(2 * rows)
    onehot = (flat_ids[:, None] == jnp.arange(count, dtype=jnp.int32)[None, :]).astype(jnp.int32)
    before = jnp.cumsum(onehot, axis=0, dtype=jnp.int32) - onehot
    slot = jnp.sum(before * onehot, axis=1, dtype=jnp.int32)
    place = flat_ids * cap + slot
    hit = place[None, :] == jnp.arange(count * cap, dtype=jnp.int32)[:, None]
    owner = jnp.arange(2 * rows, dtype=jnp.int32) // 2
    source = jnp.sum(jnp.where(hit, owner[None, :], 0), axis=1, dtype=jnp.int32)
    filled = jnp.any(hit, axis=1)
    gate_local = expert_gate[0]
    up_local = expert_up[0]
    rows_all = lax.all_gather(settled, "tp", axis=1, tiled=True)
    send = jnp.where(filled[:, None], rows_all[source], jnp.zeros((), jnp.bfloat16)).reshape(
        count, cap, -1
    )
    arrived = lax.all_to_all(send, "sp", split_axis=0, concat_axis=0, tiled=True)
    flat = arrived.reshape(count * cap, -1)
    gate = jnp.dot(flat, gate_local, preferred_element_type=jnp.float32)
    up = jnp.dot(flat, up_local, preferred_element_type=jnp.float32)
    hidden = (jax.nn.silu(gate) * up).astype(jnp.bfloat16)
    partial_value = jnp.dot(hidden, expert_down[0], preferred_element_type=jnp.float32).reshape(
        count, cap, -1
    )
    summed = summed_on_arrival(partial_value.astype(jnp.bfloat16), "tp", 2).astype(jnp.bfloat16)
    back = lax.all_to_all(summed, "sp", split_axis=0, concat_axis=0, tiled=True).reshape(
        count * cap, -1
    )
    picked = back[place].reshape(rows, 2, -1).astype(jnp.float32)
    routed = route_weight[:, 0:1] * picked[:, 0] + route_weight[:, 1:2] * picked[:, 1]
    second = depth_scale * settled.astype(jnp.float32) + routed
    sums_two = together((jnp.sum(second, axis=1), jnp.sum(second * second, axis=1)), "tp")
    return finish_norm(second, sums_two, gain_final, bias_final, columns)


def solution(mesh):
    in_specs = (
        P("sp", "tp"),
        P("sp", "tp"),
        P("sp", "tp", None),
        P("sp", "tp"),
        P("tp"),
        P("sp", "tp"),
        P("sp", "tp", None),
        P("sp", "tp"),
        P("tp"),
        P("tp", None),
        P("tp", None),
        P("tp"),
        P("tp"),
        P("sp", None),
        P("sp", None),
        P("sp", None, "tp"),
        P("sp", None, "tp"),
        P("sp", "tp", None),
        P("tp"),
        P("tp"),
    )
    out_specs = P("sp", "tp")
    return jax.shard_map(body, mesh=mesh, in_specs=in_specs, out_specs=out_specs, check_vma=False)
```

profile of v0, /device:TPU:1, one launch (start us, length us, event | category | flops | bytes accessed | tf_op | source)
XLA Modules:
  0.0 525.0 jit_solution(11694092158620046760)
XLA Ops:
  6.5 1.0 copy.109
  7.5 1.4 pad_maximum_fusion
  9.7 44.4 %all_gather.14 = f32[4096,3]{0,1:T(4,128)S(1)} all-gather(f32[128,3]{0,1:T(4,128)S(1)} %pad_maximum_fusion.1), channel_id=1, replica_groups=mesh['sp'=32,'tp'=16] {'sp'}, dimensions={0}, use_global_device_ids=true | all-gather | bytes 50688 | tf_op jit(solution)/shard_map/all_gather | solution.py:32
  55.0 42.4 %all-gather.3.cloned.1.call-done = bf16[1572864]{0:T(1024)(128)(2,1)} async-done(((bf16[49152]{0:T(1024)(128)(2,1)}), bf16[1572864]{0:T(1024)(128)(2,1)}) %all-gather.3.cloned.1.call-update) | async-done | bytes 3145744 | tf_op jit(solution)/shard_map/all_gather | solution.py:18
  97.4 4.8 reshape.355
  102.2 2.3 slice.88
  104.5 1.6 slice-done
  106.1 2.4 reshape_reshape.7
  108.5 1.6 reshape_reshape.6
  110.7 7.6 %while.19 = (s32[]{:T(128)}, f32[128,1,2,64]{0,3,2,1:T(8,128)S(1)}, f32[128,1,1,128]{0,3,2,1:T(8,128)S(1)}, f32[1,2,128]{2,1,0:T(2,128)S(1)}, f32[1,1,128]{2,1,0...) while((s32[]{:T(128)}, f32[128,1,2,64]{0,3,2,1:T(8,128)S(1)}, ...), condition=%wide.region_7.8_spmd, body=%wide.region_0.7_spmd.sunk | while | flops 24576268 | bytes 1671629 | solution.py:168
  110.7 6.1 %conditional.2 = ((f32[128,1,2,64]{0,3,2,1:T(8,128)S(1)}, f32[128,1,1,128]{0,3,2,1:T(8,128)S(1)}, f32[1,2,128]{2,1,0:T(2,128)S(1)}, f32[1,1,128]{2,1,0:T(1,128)S(1)})) conditional(s32[]{:T(128)} %convert_element_type.122, (f32[128,1,2,64]{0,3,2,1:T(8,128)S(1)}, f32[128,1,1,128]{0,3,2,1:T(8,128)S(1)}, f32[1,2,128]{2,1,0:T(2,128)S(1)}, ...), branch_computations={%region_1.0_spmd, %region_2.6_spmd} | conditional | flops 24576264 | bytes 1671338 | solution.py:146
  110.9 1.0 fusion.37
  111.8 1.1 reduce_window_sum.40
  113.0 1.0 fusion.4
  114.3 2.2 reduce_window_sum.39
  118.4 18.7 %all_to_all.38 = f32[16,1,256]{2,1,0:T(1,128)S(1)} all-to-all(f32[16,1,256]{2,1,0:T(1,128)S(1)} %broadcast_in_dim.95), channel_id=1, replica_groups=mesh['sp'=32,'tp'=16] {'tp'}, dimensions={0} | all-to-all | bytes 32768 | tf_op jit(solution)/shard_map/all_to_all | solution.py:37
  138.9 3.8 all-to-all-start.1
  144.4 15.6 %all-to-all-done.1 = bf16[16,128,128]{2,1,0:T(8,128)(2,1)S(1)} async-done(((bf16[16,128,128]{2,1,0:T(8,128)(2,1)}), bf16[16,128,128]{2,1,0:T(8,128)(2,1)S(1)}, u32[]{:S(2)}, u32[]{:S(2)}) %all-to-all-start.1) | async-done | bytes 524320 | tf_op jit(solution)/shard_map/all_to_all | solution.py:60
  160.8 3.4 all-to-all-start.2
  164.4 6.7 %all-to-all-done.2 = f32[16,1,256]{2,1,0:T(1,128)S(1)} async-done(((f32[16,1,256]{2,1,0:T(1,128)}), f32[16,1,256]{2,1,0:T(1,128)S(1)}, u32[]{:S(2)}, u32[]{:S(2)}) %all-to-all-start.2) | async-done | bytes 16416 | tf_op jit(solution)/shard_map/all_to_all | solution.py:37
  171.3 16.3 %all_gather.15 = bf16[128,2048]{1,0:T(8,128)(2,1)S(1)} all-gather(bf16[128,128]{1,0:T(8,128)(2,1)S(1)} %add_convert_fusion.1), channel_id=1, replica_groups=mesh['sp'=32,'tp'=16] {'tp'}, dimensions={1}, use_global_device_ids=true | all-gather | bytes 557056 | tf_op jit(solution)/shard_map/all_gather | solution.py:199
  187.6 3.1 gather_fusion
  190.8 2.4 gather.9
  193.3 243.2 %all_to_all.39 = bf16[32,12,2048]{2,1,0:T(8,128)(2,1)S(1)} all-to-all(bf16[32,12,2048]{2,1,0:T(8,128)(2,1)S(1)} %broadcast_select_fusion), channel_id=1, replica_groups=mesh['sp'=32,'tp'=16] {'sp'}, dimensions={0} | all-to-all | bytes 3145728 | tf_op jit(solution)/shard_map/all_to_all | solution.py:203
  436.6 1.3 reshape.335
  437.9 2.4 fusion.46
  441.6 1.6 copy.115
  443.2 5.9 %all-to-all-start.4 = ((bf16[16,32,12,128]{3,1,2,0:T(8,128)(2,1)}), bf16[16,32,12,128]{3,1,2,0:T(8,128)(2,1)S(1)}, u32[]{:S(2)}, u32[]{:S(2)}) async-start(bf16[16,32,12,128]{3,1,2,0:T(8,128)(2,1)} %bitcast.160), calls=%async_computation.4 | async-start | bytes 3145728 | tf_op jit(solution)/shard_map/all_to_all | solution.py:60
  449.5 38.2 %all-to-all-done.4 = bf16[16,32,12,128]{3,1,2,0:T(8,128)(2,1)S(1)} async-done(((bf16[16,32,12,128]{3,1,2,0:T(8,128)(2,1)}), bf16[16,32,12,128]{3,1,2,0:T(8,128)(2,1)S(1)}, u32[]{:S(2)}, u32[]{:S(2)}) %all-to-all-start.4) | async-done | bytes 1572896 | tf_op jit(solution)/shard_map/all_to_all | solution.py:60
  488.6 5.3 %all-to-all-start.5 = ((bf16[32,12,128]{2,1,0:T(8,128)(2,1)}), bf16[32,12,128]{2,1,0:T(8,128)(2,1)S(1)}, u32[]{:S(2)}, u32[]{:S(2)}) async-start(bf16[32,12,128]{2,1,0:T(8,128)(2,1)} %copy.88), calls=%async_computation.5 | async-start | bytes 262144 | tf_op jit(solution)/shard_map/all_to_all | solution.py:212
  493.9 10.3 %all-to-all-done.5 = bf16[32,12,128]{2,1,0:T(8,128)(2,1)S(1)} async-done(((bf16[32,12,128]{2,1,0:T(8,128)(2,1)}), bf16[32,12,128]{2,1,0:T(8,128)(2,1)S(1)}, u32[]{:S(2)}, u32[]{:S(2)}) %all-to-all-start.5) | async-done | bytes 98336 | tf_op jit(solution)/shard_map/all_to_all | solution.py:212
  505.4 12.0 %all_to_all.40 = f32[16,1,256]{2,1,0:T(1,128)S(1)} all-to-all(f32[16,1,256]{2,1,0:T(1,128)S(1)} %broadcast_in_dim.102), channel_id=1, replica_groups=mesh['sp'=32,'tp'=16] {'tp'}, dimensions={0} | all-to-all | bytes 32768 | tf_op jit(solution)/shard_map/all_to_all | solution.py:37
  (134 shorter events, 12.6 us)
Async XLA Ops:
  6.5 434.5 %copy-start = (bf16[1,256,2048]{2,1,0:T(8,128)(2,1)S(1)}, bf16[1,256,2048]{2,1,0:T(8,128)(2,1)}, u32[]{:S(2)}) copy-start(bf16[1,256,2048]{2,1,0:T(8,128)(2,1)} %param.41) | copy-start | bytes 3145732
  6.5 90.9 %all-gather.3.cloned.1.call-start = ((), (), s32[]{:S(2)}) async-start(), calls=%async_computation.7 | async-start | bytes 3244032 | tf_op jit(solution)/shard_map/all_gather | solution.py:18
  104.5 1.6 slice-start
  108.5 2.2 copy-start.14
  110.6 26.5 %copy-start.7 = (f32[128]{0:T(128)S(1)}, f32[128]{0:T(128)}, u32[]{:S(2)}) copy-start(f32[128]{0:T(128)} %param.28) | copy-start | bytes 1540
  110.7 26.6 %copy-start.2 = (bf16[128,2048]{1,0:T(8,128)(2,1)S(1)}, bf16[128,2048]{1,0:T(8,128)(2,1)}, u32[]{:S(2)}) copy-start(bf16[128,2048]{1,0:T(8,128)(2,1)} %param.33) | copy-start | bytes 1572868
  110.7 26.9 %copy-start.12 = (f32[128]{0:T(128)S(1)}, f32[128]{0:T(128)}, u32[]{:S(2)}) copy-start(f32[128]{0:T(128)} %param.32) | copy-start | bytes 1540
  118.3 19.3 %copy-start.3 = (bf16[128,2048]{1,0:T(8,128)(2,1)S(1)}, bf16[128,2048]{1,0:T(8,128)(2,1)}, u32[]{:S(2)}) copy-start(bf16[128,2048]{1,0:T(8,128)(2,1)} %param.34) | copy-start | bytes 1572868
  137.6 5.1 copy-start.5
  137.6 22.5 %copy-start.4 = (bf16[128,128]{1,0:T(8,128)(2,1)S(1)}, bf16[128,128]{1,0:T(8,128)(2,1)}, u32[]{:S(2)}) copy-start(bf16[128,128]{1,0:T(8,128)(2,1)} %param.24) | copy-start | bytes 98308
  138.0 33.2 %copy-start.8 = (f32[128]{0:T(128)S(1)}, f32[128]{0:T(128)}, u32[]{:S(2)}) copy-start(f32[128]{0:T(128)} %param.36) | copy-start | bytes 1540
  138.0 33.2 %copy-start.9 = (f32[128]{0:T(128)S(1)}, f32[128]{0:T(128)}, u32[]{:S(2)}) copy-start(f32[128]{0:T(128)} %param.35) | copy-start | bytes 1540
  138.9 21.1 %all-to-all-start.1 = ((bf16[16,128,128]{2,1,0:T(8,128)(2,1)}), bf16[16,128,128]{2,1,0:T(8,128)(2,1)S(1)}, u32[]{:S(2)}, u32[]{:S(2)}) async-start(bf16[16,128,128]{2,1,0:T(8,128)(2,1)} %bitcast.159), calls=%async_computation.1 | async-start | bytes 1048576 | tf_op jit(solution)/shard_map/all_to_all | solution.py:60
  160.8 10.3 %all-to-all-start.2 = ((f32[16,1,256]{2,1,0:T(1,128)}), f32[16,1,256]{2,1,0:T(1,128)S(1)}, u32[]{:S(2)}, u32[]{:S(2)}) async-start(f32[16,1,256]{2,1,0:T(1,128)} %broadcast_in_dim.96), calls=%async_computation.2 | async-start | bytes 32768 | tf_op jit(solution)/shard_map/all_to_all | solution.py:37
  437.9 2.4 copy-start.1
  437.9 2.5 copy-start.13
  443.2 50.7 %copy-start.6 = (f32[128,2]{0,1:T(2,128)S(1)}, f32[128,2]{0,1:T(2,128)}, u32[]{:S(2)}) copy-start(f32[128,2]{0,1:T(2,128)} %param.38) | copy-start | bytes 3076
  443.2 44.5 %all-to-all-start.4 = ((bf16[16,32,12,128]{3,1,2,0:T(8,128)(2,1)}), bf16[16,32,12,128]{3,1,2,0:T(8,128)(2,1)S(1)}, u32[]{:S(2)}, u32[]{:S(2)}) async-start(bf16[16,32,12,128]{3,1,2,0:T(8,128)(2,1)} %bitcast.160), calls=%async_computation.4 | async-start | bytes 3145728 | tf_op jit(solution)/shard_map/all_to_all | solution.py:60
  449.1 68.3 %copy-start.10 = (f32[128]{0:T(128)S(1)}, f32[128]{0:T(128)}, u32[]{:S(2)}) copy-start(f32[128]{0:T(128)} %param.43) | copy-start | bytes 1540
  449.2 68.3 %copy-start.11 = (f32[128]{0:T(128)S(1)}, f32[128]{0:T(128)}, u32[]{:S(2)}) copy-start(f32[128]{0:T(128)} %param.42) | copy-start | bytes 1540
  488.6 15.6 %all-to-all-start.5 = ((bf16[32,12,128]{2,1,0:T(8,128)(2,1)}), bf16[32,12,128]{2,1,0:T(8,128)(2,1)S(1)}, u32[]{:S(2)}, u32[]{:S(2)}) async-start(bf16[32,12,128]{2,1,0:T(8,128)(2,1)} %copy.88), calls=%async_computation.5 | async-start | bytes 262144 | tf_op jit(solution)/shard_map/all_to_all | solution.py:212
Sparse Core Ops, SparseCore 0:
  10.5 86.8 all-gather.2
where the time goes:
time: 530 us; the launch traced here: 525 us
  blocking collectives  335 us (63%)
  waiting for transfers between devices  113 us (21%)
  local copies, waits for them, and re-layouts  27.7 us (5%)
  starting transfers between devices  18.4 us (3%)
  between operations  13.9 us (3%)
  other arithmetic  8.59 us (2%)
  matrix products  6.88 us (1%)
    all_to_all x1, blocking collectives, body(): lax.all_to_all(send, 'sp', split_axis=0, concat_axis=0, tiled=True)  243 us
    all_to_all x2, waiting for transfers between devices, summed_on_arrival(): parts = lax.all_to_all(split_up(shard, dim, length), axis, 0, 0, tiled=True)  53.8 us
    all_gather x1, blocking collectives, sent_together(): lax.all_gather(both, axis, axis=dim, tiled=True)  44.4 us
    all_gather x1, waiting for transfers between devices, gather_packed(): lines, at, finished = (lax.all_gather(flat, axis), 0, [])  42.4 us
    all_to_all x2, blocking collectives, sent_to_all(): return lax.all_to_all(copies, axis, split_axis=0, concat_axis=0, tiled=True)  30.7 us
    all_gather x1, blocking collectives, body(): rows_all = lax.all_gather(settled, 'tp', axis=1, tiled=True)  16.3 us
  transfers between devices with their start and end apart: 5, of which 5 were waited for; matrix products, arithmetic and copies ran while one was open for 1% of the time, Pallas kernels for 0%

commit v1 on v0

v1 whole, which is shorter than its diff:
```python
import functools
import jax
import jax.numpy as jnp
from jax import lax
from jax.experimental import pallas as pl
from jax.experimental.pallas import tpu as pltpu
from jax.sharding import PartitionSpec as P

depth_scale = 2.0**0.5
norm_eps = 1e-05
MESH = pl.DeviceIdType.MESH
NX = 4
CAP = 12
STRIDE = 16
bf16 = jnp.bfloat16
f32 = jnp.float32


def iota(shape, dim):
    return lax.broadcasted_iota(jnp.int32, shape, dim)


def ones_where(cond):
    return jnp.where(cond, 1.0, 0.0).astype(bf16)


def dot(a, b):
    return jnp.dot(a, b, preferred_element_type=f32)


def dot_tr(a, b):
    return lax.dot_general(a, b, (((1,), (1,)), ((), ())), preferred_element_type=f32)


def dot_tl(a, b):
    return lax.dot_general(a, b, (((0,), (0,)), ((), ())), preferred_element_type=f32)


def split(v, pieces):
    found = []
    for _ in range(pieces):
        part = v.astype(bf16)
        found.append(part)
        v = v - part.astype(f32)
    return found


def spread(rows8, low, high):
    parts = [p.astype(f32) for p in split(rows8, 3)] + [jnp.zeros_like(rows8)]
    stacked = jnp.concatenate(parts, axis=0).astype(bf16)
    row = iota((32, 256), 0)
    lane = iota((32, 256), 1)
    slot = row & 7
    pick = jnp.zeros((32, 256), jnp.bool_)
    for r, (first, last) in zip(low, high):
        pick = pick | ((slot == r) & (lane >= first) & (lane < last) & (row < 24))
    return dot_tl(stacked, ones_where(pick))


def rowsums(v):
    cat = jnp.concatenate(split(v, 3), axis=1)
    lane = iota((8, 768), 1) & 255
    row = iota((8, 768), 0)
    return dot_tr(ones_where((lane < 128) == (row < 4)), cat)


def rcopy(src, dst, send, recv, sp, tp):
    return pltpu.make_async_remote_copy(
        src_ref=src, dst_ref=dst, send_sem=send, recv_sem=recv, device_id=(sp, tp), device_id_type=MESH
    )


def loop(low, high, step):
    def run(i, carry):
        step(i)
        return carry

    lax.fori_loop(low, high, run, 0)


def attend_kernel(
    nz, qa_ref, qb_ref, ka_ref, kb_ref, off_ref, out_ref,
    kva, kvr, kvb, off, qba, qbb, ret, back, tot, tback,
    ks, kr, qs, qr, rs, rr,
):
    sp, tp = lax.axis_index("sp"), lax.axis_index("tp")
    z, x = lax.div(sp, NX), lax.rem(sp, NX)

    barrier = pltpu.get_barrier_semaphore()

    def greet_x(d):
        pl.semaphore_signal(barrier, 1, device_id=(z * NX + lax.rem(x + d, NX), tp), device_id_type=MESH)

    def greet_z(d):
        pl.semaphore_signal(barrier, 1, device_id=(lax.rem(z + d, nz) * NX + x, tp), device_id_type=MESH)

    loop(1, NX, greet_x)
    loop(1, nz, greet_z)
    pl.semaphore_wait(barrier, NX - 1 + nz - 1)

    def key_copies(d, src_x):
        peer = z * NX + lax.rem(x + d, NX)
        rows = pl.ds(pl.multiple_of(src_x * 128, 128), 128)
        return (
            rcopy(ka_ref, kva.at[rows, :], ks.at[0, d], kr.at[0, d], peer, tp),
            rcopy(kb_ref, kvb.at[rows, :], ks.at[1, d], kr.at[1, d], peer, tp),
            rcopy(off_ref, off.at[:, rows], ks.at[2, d], kr.at[2, d], peer, tp),
        )

    def query_copies(dst_z, src_z):
        peer = dst_z * NX + x
        return (
            rcopy(qa_ref, qba.at[src_z], qs.at[0, dst_z], qr.at[0, src_z], peer, tp),
            rcopy(qb_ref, qbb.at[src_z], qs.at[1, dst_z], qr.at[1, src_z], peer, tp),
        )

    def result_copies(dst_z, src_z):
        peer = dst_z * NX + x
        return (
            rcopy(ret.at[dst_z], back.at[src_z], rs.at[0, dst_z], rr.at[0, src_z], peer, tp),
            rcopy(tot.at[dst_z], tback.at[src_z], rs.at[1, dst_z], rr.at[1, src_z], peer, tp),
        )

    def send_keys(d):
        for c in key_copies(d, x):
            c.start()

    loop(1, NX, send_keys)

    def send_query(k):
        for c in query_copies(z - 1 - k, z):
            c.start()

    loop(0, z, send_query)

    mine = pl.ds(pl.multiple_of(x * 128, 128), 128)
    kva[mine, :] = ka_ref[...]
    kvb[mine, :] = kb_ref[...]
    off[:, mine] = off_ref[...]
    qba[z] = qa_ref[...]
    qbb[z] = qb_ref[...]

    def await_keys(d):
        for c in key_copies(d, lax.rem(x - d + NX, NX)):
            c.wait_recv()

    loop(1, NX, await_keys)
    keys_a = kva[...]
    kvr[...] = pltpu.roll(keys_a.astype(f32), 64, 1).astype(bf16)

    lane = iota((128, 128), 1)
    gap = lane - iota((128, 128), 0)
    r256, c256 = iota((256, 256), 0) & 127, iota((256, 256), 1)
    later_matrix = ones_where((r256 > c256) | (c256 >= 128))
    ones8 = jnp.ones((8, 256), bf16)
    row8 = iota((8, 128), 0)

    def visit(zq):
        @pl.when(zq > z)
        def _():
            for c in query_copies(z, zq):
                c.wait_recv()

        qa, qb = qba[zq], qbb[zq]
        zero = jnp.zeros_like(qa)
        accs, totals = [], []
        for h in range(3):
            q = (jnp.where(lane < 64, qa, zero), jnp.where(lane >= 64, qa, zero), qb)[h]
            scale = (64.0**-0.5, 64.0**-0.5, 128.0**-0.5)[h]
            gone = jnp.zeros((128, 128), f32)
            total = jnp.zeros((8, 128), f32)
            weights = [None] * NX
            for b in reversed(range(NX)):
                rows = slice(b * 128, b * 128 + 128)
                keys = (kva[rows, :], kvr[rows, :], kvb[rows, :128])[h]
                scores = dot_tr(q, keys) * scale + off[h : h + 1, rows]
                valid = gap < (zq - z) * (NX * 128) + (x - b) * 128
                soft = jnp.maximum(scores, 0.0) + jnp.log(1.0 + jnp.exp(-jnp.abs(scores)))
                cat = jnp.concatenate(split(jnp.where(valid, soft, 0.0), 2), axis=1)
                sums = dot(cat, later_matrix)
                total = total + dot_tr(ones8, cat)
                power = (scores - soft) - (sums[:, :128] + gone)
                gone = gone + sums[:, 128:]
                weights[b] = jnp.where(valid, jnp.exp(power), 0.0).astype(bf16)
            values = (kvr[...], kva[...], kvb[:, 128:])[h]
            accs.append(dot(jnp.concatenate(weights, axis=1), values))
            totals.append(total)
        both = jnp.where(lane < 64, accs[0], accs[1])
        found = jnp.concatenate([both, accs[2]], axis=1).astype(bf16)
        sums8 = jnp.where(row8 == 0, totals[0], jnp.where(row8 == 1, totals[1], totals[2]))

        @pl.when(zq == z)
        def _():
            back[z] = found
            tback[z] = sums8

        @pl.when(zq > z)
        def _():
            ret[zq] = found
            tot[zq] = sums8
            for c in result_copies(zq, z):
                c.start()

    loop(z, nz, visit)

    def gather(k, carry):
        acc, gone = carry
        zk = z - k

        @pl.when(k > 0)
        def _():
            for c in result_copies(z, zk):
                c.wait_recv()

        wide = spread(jnp.exp(-gone), (0, 1, 2), ((0, 64), (64, 128), (128, 256)))
        return acc + wide * back[zk].astype(f32), gone + tback[zk]

    acc, _ = lax.fori_loop(
        0, z + 1, gather, (jnp.zeros((128, 256), f32), jnp.zeros((8, 128), f32))
    )
    out_ref[...] = acc

    def end_keys(d):
        for c in key_copies(d, x):
            c.wait_send()

    def end_query(k):
        for c in query_copies(z - 1 - k, z):
            c.wait_send()

    def end_result(zq):
        for c in result_copies(zq, z):
            c.wait_send()

    loop(1, NX, end_keys)
    loop(0, z, end_query)
    loop(z + 1, nz, end_result)


def near_order(n):
    return sorted(range(1, n), key=lambda d: (min(d, n - d), d))


def layer_kernel(
    nsp, ntp,
    att_ref, res_ref, ga_ref, gb_ref, gs_ref, bs_ref, gf_ref, bf_ref, ids_ref, route_ref,
    pa_hbm, pb_hbm, wg_hbm, wu_hbm, wd_hbm, out_ref,
    pa, pb, wg, wu, wd, wsem,
    stat, stats, ss, sr,
    p1s, p1o, p1v, p1r, p1i, p1ss, p1sr, p1rs, p1rr,
    dsp, drv, ds_, dr_,
    xg, gs2, gr2, fs2, fr2, acc_g, acc_u,
    p2s, p2o, p2v, p2r, p2i, p2ss, p2sr, p2rs, p2rr,
    rts, rtv, ts_, tr_,
):
    sp, tp = lax.axis_index("sp"), lax.axis_index("tp")
    ny = ntp // 2
    y, c = lax.div(tp, 2), lax.rem(tp, 2)
    mate = y * 2 + 1 - c
    columns = ntp * 128

    loads = [
        pltpu.make_async_copy(src, dst, wsem.at[i])
        for i, (src, dst) in enumerate(
            ((pa_hbm, pa), (pb_hbm, pb), (wg_hbm, wg), (wu_hbm, wu), (wd_hbm, wd))
        )
    ]
    for load in loads:
        load.start()

    barrier = pltpu.get_barrier_semaphore()

    def greet_sp(d):
        pl.semaphore_signal(barrier, 1, device_id=(lax.rem(sp + d, nsp), tp), device_id_type=MESH)

    def greet_tp(d):
        pl.semaphore_signal(barrier, 1, device_id=(sp, lax.rem(tp + d, ntp)), device_id_type=MESH)

    loop(1, nsp, greet_sp)
    loop(1, ntp, greet_tp)
    pl.semaphore_wait(barrier, nsp - 1 + ntp - 1)

    def stat_copy(n, d):
        return rcopy(stat.at[n], stats.at[n, d], ss.at[n, d], sr.at[n, d], sp, lax.rem(tp + d, ntp))

    def over_tp(n, rows8):
        stat[n] = rows8
        loop(1, ntp, lambda d: stat_copy(n, d).start())
        loop(1, ntp, lambda d: stat_copy(n, d).wait_recv())
        total = rows8
        for d in range(1, ntp):
            total = total + stats[n, d]
        return total

    def summed(product, sent, own, from_mate, reduced, arrived, sem_ms, sem_mr, sem_s, sem_r):
        def to_mate(d):
            return rcopy(sent.at[d], from_mate.at[d], sem_ms.at[d], sem_mr.at[d], sp, mate)

        def to_chip(d):
            return rcopy(
                reduced.at[d], arrived.at[d], sem_s.at[d], sem_r.at[d], sp, lax.rem(y + d, ny) * 2 + c
            )

        def make(d):
            both = product(lax.rem(y + d, ny))
            left, right = both[:, :128], both[:, 128:]
            sent[d] = jnp.where(c == 0, right, left).astype(bf16)
            to_mate(d).start()
            own[d] = jnp.where(c == 0, left, right)

        def pass_on(d):
            to_mate(d).wait_recv()
            reduced[d] = (own[d] + from_mate[d].astype(f32)).astype(bf16)
            to_chip(d).start()

        order = near_order(ny)[::-1]
        make(order[0])
        for before, d in zip(order, order[1:] + [0]):
            make(d)
            pass_on(before)
        to_mate(0).wait_recv()
        total = own[0] + from_mate[0].astype(f32)
        for d in order[::-1]:
            to_chip(d).wait_recv()
            total = total + arrived[d].astype(f32)
        return total, to_mate, to_chip

    lane128 = iota((128, 128), 1)
    hot = [ids_ref[:, k : k + 1] == lane128 for k in range(2)]
    tri = ones_where(iota((128, 128), 0) > lane128)
    earlier = dot(tri, ones_where(hot[0] | hot[1]))
    lane_all = iota((128, nsp * STRIDE), 1).astype(f32)
    choice = []
    for k in range(2):
        slot = jnp.sum(jnp.where(hot[k], earlier, 0.0), axis=1, keepdims=True)
        place = ids_ref[:, k : k + 1].astype(f32) * float(STRIDE) + slot
        choice.append(ones_where(place == lane_all))
    row_c, col_c = iota((nsp * CAP, nsp * STRIDE), 0), iota((nsp * CAP, nsp * STRIDE), 1)
    block_c = (row_c * (-(-(1 << 17) // CAP))) >> 17
    compact = ones_where(col_c == row_c + block_c * (STRIDE - CAP))

    attend = att_ref[...]
    squares = over_tp(0, rowsums(attend * attend))
    halves = ((0, 128), (128, 256))
    scale = spread(lax.rsqrt(squares / float(columns) + norm_eps), (0, 4), halves)
    normed_a = (attend[:, :128] * scale[:, :128] * ga_ref[...]).astype(bf16)
    normed_b = (attend[:, 128:] * scale[:, 128:] * gb_ref[...]).astype(bf16)
    loads[0].wait()
    loads[1].wait()

    def project(yy):
        cols = pl.ds(pl.multiple_of(yy * 256, 256), 256)
        return dot(normed_a, pa[:, cols]) + dot(normed_b, pb[:, cols])

    mixed, to_mate1, to_chip1 = summed(project, p1s, p1o, p1v, p1r, p1i, p1ss, p1sr, p1rs, p1rr)
    first = depth_scale * res_ref[...].astype(f32) + mixed.astype(bf16).astype(f32)

    row8 = iota((8, 128), 0)

    def norm(n, total, gain, bias):
        sums = over_tp(n, rowsums(jnp.concatenate([total, total * total], axis=1)))
        mean = sums[0:1, :] / float(columns)
        var = sums[4:5, :] / float(columns) - mean * mean
        wide = spread(jnp.where(row8 < 4, mean, lax.rsqrt(var + norm_eps)), (0, 4), halves)
        return ((total - wide[:, :128]) * wide[:, 128:] * gain + bias).astype(bf16)

    settled = norm(1, first, gs_ref[...], bs_ref[...])

    def sp_copy(src, dst, send, recv, d):
        peer = lax.rem(sp + d, nsp)
        rows = pl.ds(pl.multiple_of(peer * STRIDE, STRIDE), STRIDE)
        here = pl.ds(pl.multiple_of(sp * STRIDE, STRIDE), STRIDE)
        return rcopy(src.at[rows, :], dst.at[here, :], send.at[d], recv.at[d], peer, tp)

    def sp_await(src, dst, send, recv, d):
        peer = lax.rem(sp - d + nsp, nsp)
        rows = pl.ds(pl.multiple_of(peer * STRIDE, STRIDE), STRIDE)
        rcopy(src.at[rows, :], dst.at[rows, :], send.at[d], recv.at[d], peer, tp).wait_recv()

    here = pl.ds(pl.multiple_of(sp * STRIDE, STRIDE), STRIDE)

    def exchange(src, dst, send, recv, value):
        src[...] = value
        loop(1, nsp, lambda d: sp_copy(src, dst, send, recv, d).start())
        dst[here, :] = src[here, :]
        loop(1, nsp, lambda d: sp_await(src, dst, send, recv, d))
        return dst[...]

    arrived = exchange(dsp, drv, ds_, dr_, dot_tl(choice[0] + choice[1], settled).astype(bf16))
    tokens = dot(compact, arrived).astype(bf16)

    side = pl.ds(pl.multiple_of(c * 128, 128), 128)
    mate_side = pl.ds(pl.multiple_of((1 - c) * 128, 128), 128)

    def to_same(d):
        block = xg.at[y, :, side]
        return rcopy(block, block, gs2.at[d], gr2.at[d], sp, lax.rem(y + d, ny) * 2 + c)

    def await_same(d):
        block = xg.at[lax.rem(y - d + ny, ny), :, side]
        rcopy(block, block, gs2.at[d], gr2.at[d], sp, lax.rem(y - d + ny, ny) * 2 + c).wait_recv()

    def hand_over(d):
        block = xg.at[lax.rem(y - d + ny, ny), :, side]
        return rcopy(block, block, fs2.at[d], fr2.at[d], sp, mate)

    def await_mate(d):
        block = xg.at[lax.rem(y - d + ny, ny), :, mate_side]
        rcopy(block, block, fs2.at[d], fr2.at[d], sp, mate).wait_recv()

    def take(d, start):
        yy = lax.rem(y - d + ny, ny)
        rows = pl.ds(pl.multiple_of(yy * 256, 256), 256)
        block = xg[yy]
        gate, up = dot(block, wg[rows, :]), dot(block, wu[rows, :])
        if start:
            acc_g[...] = gate
            acc_u[...] = up
        else:
            acc_g[...] += gate
            acc_u[...] += up

    xg[y, :, side] = tokens
    order = near_order(ny)
    hand_over(0).start()
    for d in order:
        to_same(d).start()
    loads[2].wait()
    loads[3].wait()
    before = 0
    for d in order:
        await_same(d)
        hand_over(d).start()
        await_mate(before)
        take(before, before == 0)
        before = d
    await_mate(before)
    take(before, False)

    gate = acc_g[...]
    hidden = (gate / (1.0 + jnp.exp(-gate)) * acc_u[...]).astype(bf16)
    loads[4].wait()

    def down(yy):
        return dot(hidden, wd[:, pl.ds(pl.multiple_of(yy * 256, 256), 256)])

    outputs, to_mate2, to_chip2 = summed(down, p2s, p2o, p2v, p2r, p2i, p2ss, p2sr, p2rs, p2rr)

    returned = exchange(rts, rtv, ts_, tr_, dot_tl(compact, outputs.astype(bf16)).astype(bf16))
    routed = route_ref[:, 0:1] * dot(choice[0], returned) + route_ref[:, 1:2] * dot(choice[1], returned)
    second = depth_scale * settled.astype(f32) + routed
    out_ref[...] = norm(2, second, gf_ref[...], bf_ref[...])

    for n in range(3):
        loop(1, ntp, lambda d, n=n: stat_copy(n, d).wait_send())
    for to_mate, to_chip in ((to_mate1, to_chip1), (to_mate2, to_chip2)):
        loop(0, ny, lambda d, f=to_mate: f(d).wait_send())
        loop(1, ny, lambda d, f=to_chip: f(d).wait_send())
    loop(1, nsp, lambda d: sp_copy(dsp, drv, ds_, dr_, d).wait_send())
    loop(1, nsp, lambda d: sp_copy(rts, rtv, ts_, tr_, d).wait_send())
    loop(1, ny, lambda d: to_same(d).wait_send())
    loop(0, ny, lambda d: hand_over(d).wait_send())


def body(
    nsp, ntp,
    residual_in, query_alpha, pairs_alpha, offset_alpha, gain_alpha,
    query_beta, pairs_beta, offset_beta, gain_beta, project_alpha, project_beta,
    gain_settle, bias_settle, expert_ids, route_weight,
    expert_gate, expert_up, expert_down, gain_final, bias_final,
):
    nz, ny = nsp // NX, ntp // 2
    vmem = pl.BlockSpec(memory_space=pltpu.VMEM)
    hbm = pl.BlockSpec(memory_space=pl.ANY)
    dma = pltpu.SemaphoreType.DMA
    V = pltpu.VMEM
    offsets = jnp.concatenate([offset_alpha.T, offset_beta.T, jnp.zeros((5, 128), f32)], axis=0)
    attend = pl.pallas_call(
        functools.partial(attend_kernel, nz),
        out_shape=jax.ShapeDtypeStruct((128, 256), f32),
        in_specs=[vmem] * 5,
        out_specs=vmem,
        scratch_shapes=[
            V((NX * 128, 128), bf16), V((NX * 128, 128), bf16), V((NX * 128, 256), bf16),
            V((8, NX * 128), f32), V((nz, 128, 128), bf16), V((nz, 128, 128), bf16),
            V((nz, 128, 256), bf16), V((nz, 128, 256), bf16), V((nz, 8, 128), f32), V((nz, 8, 128), f32),
            dma((3, NX)), dma((3, NX)), dma((2, nz)), dma((2, nz)), dma((2, nz)), dma((2, nz)),
        ],
        compiler_params=pltpu.CompilerParams(
            collective_id=0, has_side_effects=True, vmem_limit_bytes=32 * 1024 * 1024
        ),
        name="attend",
    )(query_alpha, query_beta, pairs_alpha.reshape(128, 128), pairs_beta.reshape(128, 256), offsets)

    rows = nsp * CAP
    wide = nsp * STRIDE

    def sum_scratch(height):
        return [
            V((ny, height, 128), bf16), V((ny, height, 128), f32), V((ny, height, 128), bf16),
            V((ny, height, 128), bf16), V((ny, height, 128), bf16),
            dma((ny,)), dma((ny,)), dma((ny,)), dma((ny,)),
        ]

    weights = (project_alpha, project_beta, expert_gate[0], expert_up[0], expert_down[0])
    vectors = [
        v.reshape(1, 128) for v in (gain_alpha, gain_beta, gain_settle, bias_settle, gain_final, bias_final)
    ]
    return pl.pallas_call(
        functools.partial(layer_kernel, nsp, ntp),
        out_shape=jax.ShapeDtypeStruct((128, 128), bf16),
        in_specs=[vmem] * 10 + [hbm] * 5,
        out_specs=vmem,
        scratch_shapes=[V(w.shape, bf16) for w in weights]
        + [dma((5,)), V((3, 8, 128), f32), V((3, ntp, 8, 128), f32), dma((3, ntp)), dma((3, ntp))]
        + sum_scratch(128)
        + [V((wide, 128), bf16), V((wide, 128), bf16), dma((nsp,)), dma((nsp,))]
        + [
            V((ny, rows, 256), bf16), dma((ny,)), dma((ny,)), dma((ny,)), dma((ny,)),
            V((rows, expert_gate.shape[2]), f32), V((rows, expert_gate.shape[2]), f32),
        ]
        + sum_scratch(rows)
        + [V((wide, 128), bf16), V((wide, 128), bf16), dma((nsp,)), dma((nsp,))],
        compiler_params=pltpu.CompilerParams(
            collective_id=1, has_side_effects=True, vmem_limit_bytes=48 * 1024 * 1024
        ),
        name="layer",
    )(attend, residual_in, *vectors, expert_ids, route_weight, *weights)


def solution(mesh):
    in_specs = (
        P("sp", "tp"),
        P("sp", "tp"),
        P("sp", "tp", None),
        P("sp", "tp"),
        P("tp"),
        P("sp", "tp"),
        P("sp", "tp", None),
        P("sp", "tp"),
        P("tp"),
        P("tp", None),
        P("tp", None),
        P("tp"),
        P("tp"),
        P("sp", None),
        P("sp", None),
        P("sp", None, "tp"),
        P("sp", None, "tp"),
        P("sp", "tp", None),
        P("tp"),
        P("tp"),
    )
    step = functools.partial(body, mesh.shape["sp"], mesh.shape["tp"])
    return jax.shard_map(step, mesh=mesh, in_specs=in_specs, out_specs=P("sp", "tp"), check_vma=False)
```

time: 530 us -> 150 us (0.28)
  blocking collectives: 335 us -> 0 us
  Pallas kernels: 0 us -> 141 us
  waiting for transfers between devices: 113 us -> 0 us
  local copies, waits for them, and re-layouts: 27.7 us -> 7.94 us
  starting transfers between devices: 18.4 us -> 0 us
  between operations: 13.9 us -> 0.17 us
  other arithmetic: 8.59 us -> 0.07 us
  matrix products: 6.88 us -> 0 us
    all_to_all x3 -> x0, blocking collectives: 274 us -> none  [the longest x1 243 us: body(): lax.all_to_all(send, 'sp', split_axis=0, concat_axis=0, tiled=True)]
    pallas_call x0 -> x2, Pallas kernels: none -> 141 us  [the longest x1 97.7 us: body(): pl.pallas_call(functools.partial(layer_kernel, nsp, ntp), out_shape=jax.S...]
    all_to_all x4 -> x0, waiting for transfers between devices: 70.9 us -> none  [the longest x2 53.8 us: summed_on_arrival(): parts = lax.all_to_all(split_up(shard, dim, length), axis, 0, 0, tiled=True)]
    all_gather x2 -> x0, blocking collectives: 60.8 us -> none  [the longest x1 44.4 us: sent_together(): lax.all_gather(both, axis, axis=dim, tiled=True)]
    all_gather x1 -> x0, waiting for transfers between devices: 42.4 us -> none  [gather_packed(): lines, at, finished = (lax.all_gather(flat, axis), 0, [])]
    all_to_all x4 -> x0, starting transfers between devices: 18.4 us -> none  [the longest x2 9.69 us: summed_on_arrival(): parts = lax.all_to_all(split_up(shard, dim, length), axis, 0, 0, tiled=True)]
    dot_general x9 -> x0, matrix products: 6.88 us -> none  [the longest x1 2.42 us: body(): gate = jnp.dot(flat, gate_local, preferred_element_type=jnp.float32)]
    gather x3 -> x0, local copies, waits for them, and re-layouts: 6.35 us -> none  [the longest x2 5.49 us: body(): rows_all[source]]
  transfers between devices with their start and end apart: 5 -> 0, of which waited for: 5 -> 0; matrix products, arithmetic and copies ran while one was open for 1% -> 0% of each run, Pallas kernels for 0% -> 0%
where the time goes in v1:
time: 150 us
  Pallas kernels  141 us (94%)
  local copies, waits for them, and re-layouts  7.94 us (5%)
    pallas_call x1, Pallas kernels, body(): pl.pallas_call(functools.partial(layer_kernel, nsp, ntp), out_shape=jax.S...  97.7 us
    pallas_call x1, Pallas kernels, body(): pl.pallas_call(functools.partial(attend_kernel, nz), out_shape=jax.ShapeD...  43.7 us
    unnamed x43, local copies, waits for them, and re-layouts  7.86 us

profile of v1, /device:TPU:1, one launch (start us, length us, event | category | flops | bytes accessed | tf_op | source)
XLA Modules:
  0.0 149.6 jit_solution(17712773855906254890)
XLA Ops:
  0.0 0.0 copy-start.17
  0.0 0.0 copy-start.9
  0.0 0.1 pad.2.clone
  0.1 0.6 copy-done.18
  0.7 0.0 copy-done.19
  0.7 0.1 maximum_maximum_fusion.off_ref
  0.8 0.0 copy-done.16
  0.8 0.1 copy.21.ids_ref
  0.9 0.0 copy-done.17
  0.9 0.0 copy-start.7
  0.9 0.0 copy-start.8
  0.9 0.1 copy.22.route_ref
  1.0 0.0 copy-done.9
  1.0 0.6 copy-done.5
  1.6 0.0 copy-done.7
  1.6 0.0 copy-done.8
  1.7 0.0 copy-start.13
  1.7 0.0 copy-start.14
  1.7 0.0 copy-start.15
  1.7 43.7 %attend.1.att_ref = f32[128,256]{1,0:T(8,128)S(1)} custom-call(bf16[128,128]{1,0:T(8,128)(2,1)S(1)} %copy-done.7, bf16[128,128]{1,0:T(8,128)(2,1)S(1)} %copy-done.8, bf16[128,128]{1,0:T(8,128)(2,1)S(1)} %bitcast.17, bf16[128,256]{1,0:T(8,128)(2,1)S(1)} %bitcast.16, f32[8,128]{1,0:T(8,128)S(1)} %maximum_maximum_fusion.off_ref), custom_call_target="tpu_custom_call" | custom-call | tf_op jit(solution)/shard_map/attend/pallas_call | solution.py:478
  45.4 0.0 copy-done.6
  45.4 0.0 copy-done.10
  45.4 0.0 copy-done.11
  45.4 0.0 copy-done.12
  45.5 0.0 copy-start
  45.5 1.2 copy-done
  46.7 1.2 copy-done.1
  47.9 1.2 copy-done.2
  49.2 1.0 copy-done.3
  50.2 1.0 copy-done.4
  51.3 97.7 %layer.1 = bf16[128,128]{1,0:T(8,128)(2,1)S(1)} custom-call(f32[128,256]{1,0:T(8,128)S(1)} %attend.1.att_ref, bf16[128,128]{1,0:T(8,128)(2,1)S(1)} %copy-done.6, f32[1,128]{1,0:T(1,128)S(1)} %bitcast.18, f32[1,128]{1,0:T(1,128)S(1)} %bitcast.19, f32[1,128]{1,0:T(1,128)S(1)} %bitcast.20, f32[1,128]{1,0:T(1,128)S(1)} %bitcast.21, f32[1,128]{1,0:T(1,128)S(1)} %bitcast.22, ...), custom_call_target="tpu_custom_call" | custom-call | tf_op jit(solution)/shard_map/layer/pallas_call | solution.py:509
  149.0 0.6 copy.24
  (16 shorter events, 0.0 us)
Async XLA Ops:
  0.0 0.7 copy-start.18
  0.0 0.7 copy-start.19
  0.0 0.8 copy-start.16
  0.0 0.9 copy-start.17
  0.0 1.0 copy-start.9
  0.8 0.8 copy-start.5
  0.9 0.8 copy-start.7
  0.9 0.8 copy-start.8
  1.7 43.8 %copy-start.6 = (bf16[128,128]{1,0:T(8,128)(2,1)S(1)}, bf16[128,128]{1,0:T(8,128)(2,1)}, u32[]{:S(2)}) copy-start(bf16[128,128]{1,0:T(8,128)(2,1)} %res_ref.1) | copy-start | bytes 98308
  1.7 43.8 %copy-start.10 = (f32[128]{0:T(128)S(1)}, f32[128]{0:T(128)}, u32[]{:S(2)}) copy-start(f32[128]{0:T(128)} %param.24) | copy-start | bytes 1540
  1.7 43.8 %copy-start.11 = (f32[128]{0:T(128)S(1)}, f32[128]{0:T(128)}, u32[]{:S(2)}) copy-start(f32[128]{0:T(128)} %param.28) | copy-start | bytes 1540
  1.7 43.8 %copy-start.12 = (f32[128]{0:T(128)S(1)}, f32[128]{0:T(128)}, u32[]{:S(2)}) copy-start(f32[128]{0:T(128)} %param.31) | copy-start | bytes 1540
  1.7 43.8 %copy-start.13 = (f32[128]{0:T(128)S(1)}, f32[128]{0:T(128)}, u32[]{:S(2)}) copy-start(f32[128]{0:T(128)} %param.32) | copy-start | bytes 1540
  1.7 43.8 %copy-start.14 = (f32[128]{0:T(128)S(1)}, f32[128]{0:T(128)}, u32[]{:S(2)}) copy-start(f32[128]{0:T(128)} %param.38) | copy-start | bytes 1540
  1.7 43.8 %copy-start.15 = (f32[128]{0:T(128)S(1)}, f32[128]{0:T(128)}, u32[]{:S(2)}) copy-start(f32[128]{0:T(128)} %param.39) | copy-start | bytes 1540
  45.5 1.2 copy-start
  46.7 1.2 copy-start.1
  47.9 1.2 copy-start.2
  49.2 1.0 copy-start.3
  50.2 1.0 copy-start.4

commit v2 on v1

v2 whole, which is shorter than its diff:
```python
import functools
import jax
import jax.numpy as jnp
from jax import lax
from jax.experimental import pallas as pl
from jax.experimental.pallas import tpu as pltpu
from jax.sharding import PartitionSpec as P

depth_scale = 2.0**0.5
norm_eps = 1e-05
MESH = pl.DeviceIdType.MESH
NX = 4
CAP = 12
STRIDE = 16
PIECES = 4
bf16 = jnp.bfloat16
f32 = jnp.float32


def iota(shape, dim):
    return lax.broadcasted_iota(jnp.int32, shape, dim)


def ones_where(cond):
    return jnp.where(cond, 1.0, 0.0).astype(bf16)


def dot(a, b):
    return jnp.dot(a, b, preferred_element_type=f32)


def dot_tr(a, b):
    return lax.dot_general(a, b, (((1,), (1,)), ((), ())), preferred_element_type=f32)


def dot_tl(a, b):
    return lax.dot_general(a, b, (((0,), (0,)), ((), ())), preferred_element_type=f32)


def split(v, pieces):
    found = []
    for _ in range(pieces):
        part = v.astype(bf16)
        found.append(part)
        v = v - part.astype(f32)
    return found


def spread(rows8, low, high):
    parts = [p.astype(f32) for p in split(rows8, 3)] + [jnp.zeros_like(rows8)]
    stacked = jnp.concatenate(parts, axis=0).astype(bf16)
    row = iota((32, 256), 0)
    lane = iota((32, 256), 1)
    slot = row & 7
    pick = jnp.zeros((32, 256), jnp.bool_)
    for r, (first, last) in zip(low, high):
        pick = pick | ((slot == r) & (lane >= first) & (lane < last) & (row < 24))
    return dot_tl(stacked, ones_where(pick))


def rowsums(v):
    cat = jnp.concatenate(split(v, 3), axis=1)
    lane = iota((8, 768), 1) & 255
    row = iota((8, 768), 0)
    return dot_tr(ones_where((lane < 128) == (row < 4)), cat)


def rcopy(src, dst, send, recv, sp, tp):
    return pltpu.make_async_remote_copy(
        src_ref=src, dst_ref=dst, send_sem=send, recv_sem=recv, device_id=(sp, tp), device_id_type=MESH
    )


def loop(low, high, step):
    def run(i, carry):
        step(i)
        return carry

    lax.fori_loop(low, high, run, 0)


def near_order(n):
    return sorted(range(1, n), key=lambda d: (min(d, n - d), d))


def layer_kernel(
    nsp, ntp,
    qa_ref, qb_ref, ka_ref, kb_ref, oa_ref, ob_ref, res_ref, ga_ref, gb_ref, gs_ref, bs_ref, gf_ref, bf_ref,
    ids_ref, route_ref, pa_hbm, pb_hbm, wg_hbm, wu_hbm, wd_hbm, out_ref,
    pa, pb, wg, wu, wd, wsem, misc,
    kva, kvr, kvb, ofs, off, qba, qbb, ret, back, tot, tback,
    ks, kr, qs, qr, rs, rr,
    stat, stats, ss, sr,
    p1s, p1o, p1v, p1r, p1i, p1ss, p1sr, p1rs, p1rr,
    dsp, drv, ds_, dr_,
    xg, as_, ar_, hs_, hr_, acc_g, acc_u,
    p2s, p2o, p2v, p2ss, p2sr, rb_s, rb_r, rbs_, rbr_,
    rts, rtv, ts_, tr_,
):
    sp, tp = lax.axis_index("sp"), lax.axis_index("tp")
    nz, ny = nsp // NX, ntp // 2
    z, x = lax.div(sp, NX), lax.rem(sp, NX)
    y, c = lax.div(tp, 2), lax.rem(tp, 2)
    mate = y * 2 + 1 - c
    columns = ntp * 128
    ends = []

    loads = [
        pltpu.make_async_copy(src, dst, wsem.at[i])
        for i, (src, dst) in enumerate(
            ((pa_hbm, pa), (pb_hbm, pb), (wg_hbm, wg), (wu_hbm, wu), (wd_hbm, wd))
        )
    ]
    for load in loads:
        load.start()

    barrier = pltpu.get_barrier_semaphore()

    def greet_sp(d):
        pl.semaphore_signal(barrier, 1, device_id=(lax.rem(sp + d, nsp), tp), device_id_type=MESH)

    def greet_tp(d):
        pl.semaphore_signal(barrier, 1, device_id=(sp, lax.rem(tp + d, ntp)), device_id_type=MESH)

    loop(1, nsp, greet_sp)
    loop(1, ntp, greet_tp)
    ofs[...] = jnp.zeros((8, 128), f32)
    ofs[0:2, :] = oa_ref[...]
    ofs[2:3, :] = ob_ref[...]
    pl.semaphore_wait(barrier, nsp - 1 + ntp - 1)

    def key_copies(d, src_x):
        peer = z * NX + lax.rem(x + d, NX)
        rows = pl.ds(pl.multiple_of(src_x * 128, 128), 128)
        return (
            rcopy(ka_ref, kva.at[rows, :], ks.at[0, d], kr.at[0, d], peer, tp),
            rcopy(kb_ref, kvb.at[rows, :], ks.at[1, d], kr.at[1, d], peer, tp),
            rcopy(ofs, off.at[:, rows], ks.at[2, d], kr.at[2, d], peer, tp),
        )

    def query_copies(dst_z, src_z):
        peer = dst_z * NX + x
        return (
            rcopy(qa_ref, qba.at[src_z], qs.at[0, dst_z], qr.at[0, src_z], peer, tp),
            rcopy(qb_ref, qbb.at[src_z], qs.at[1, dst_z], qr.at[1, src_z], peer, tp),
        )

    def result_copies(dst_z, src_z):
        peer = dst_z * NX + x
        return (
            rcopy(ret.at[dst_z], back.at[src_z], rs.at[0, dst_z], rr.at[0, src_z], peer, tp),
            rcopy(tot.at[dst_z], tback.at[src_z], rs.at[1, dst_z], rr.at[1, src_z], peer, tp),
        )

    def send_keys(d):
        for copy in key_copies(d, x):
            copy.start()

    loop(1, NX, send_keys)

    def send_query(k):
        for copy in query_copies(z - 1 - k, z):
            copy.start()

    loop(0, z, send_query)

    mine = pl.ds(pl.multiple_of(x * 128, 128), 128)
    kva[mine, :] = ka_ref[...]
    kvb[mine, :] = kb_ref[...]
    off[:, mine] = ofs[...]
    qba[z] = qa_ref[...]
    qbb[z] = qb_ref[...]

    def await_keys(d):
        for copy in key_copies(d, lax.rem(x - d + NX, NX)):
            copy.wait_recv()

    loop(1, NX, await_keys)
    keys_a = kva[...]
    kvr[...] = pltpu.roll(keys_a.astype(f32), 64, 1).astype(bf16)

    lane = iota((128, 128), 1)
    gap = lane - iota((128, 128), 0)
    r256, c256 = iota((256, 256), 0) & 127, iota((256, 256), 1)
    later_matrix = ones_where((r256 > c256) | (c256 >= 128))
    ones8 = jnp.ones((8, 256), bf16)
    row8 = iota((8, 128), 0)

    def visit(zq):
        @pl.when(zq > z)
        def _():
            for copy in query_copies(z, zq):
                copy.wait_recv()

        qa, qb = qba[zq], qbb[zq]
        zero = jnp.zeros_like(qa)
        accs, totals = [], []
        for h in range(3):
            q = (jnp.where(lane < 64, qa, zero), jnp.where(lane >= 64, qa, zero), qb)[h]
            scale = (64.0**-0.5, 64.0**-0.5, 128.0**-0.5)[h]
            gone = jnp.zeros((128, 128), f32)
            total = jnp.zeros((8, 128), f32)
            weights = [None] * NX
            for b in reversed(range(NX)):
                rows = slice(b * 128, b * 128 + 128)
                keys = (kva[rows, :], kvr[rows, :], kvb[rows, :128])[h]
                scores = dot_tr(q, keys) * scale + off[h : h + 1, rows]
                valid = gap < (zq - z) * (NX * 128) + (x - b) * 128
                soft = jnp.maximum(scores, 0.0) + jnp.log(1.0 + jnp.exp(-jnp.abs(scores)))
                cat = jnp.concatenate(split(jnp.where(valid, soft, 0.0), 2), axis=1)
                sums = dot(cat, later_matrix)
                total = total + dot_tr(ones8, cat)
                power = (scores - soft) - (sums[:, :128] + gone)
                gone = gone + sums[:, 128:]
                weights[b] = jnp.where(valid, jnp.exp(power), 0.0).astype(bf16)
            values = (kvr[...], kva[...], kvb[:, 128:])[h]
            accs.append(dot(jnp.concatenate(weights, axis=1), values))
            totals.append(total)
        both = jnp.where(lane < 64, accs[0], accs[1])
        found = jnp.concatenate([both, accs[2]], axis=1).astype(bf16)
        sums8 = jnp.where(row8 == 0, totals[0], jnp.where(row8 == 1, totals[1], totals[2]))

        @pl.when(zq == z)
        def _():
            back[z] = found
            tback[z] = sums8

        @pl.when(zq > z)
        def _():
            ret[zq] = found
            tot[zq] = sums8
            for copy in result_copies(zq, z):
                copy.start()

    loop(z, nz, visit)

    def gather(k, carry):
        acc, gone = carry
        zk = z - k

        @pl.when(k > 0)
        def _():
            for copy in result_copies(z, zk):
                copy.wait_recv()

        wide = spread(jnp.exp(-gone), (0, 1, 2), ((0, 64), (64, 128), (128, 256)))
        return acc + wide * back[zk].astype(f32), gone + tback[zk]

    attend, _ = lax.fori_loop(
        0, z + 1, gather, (jnp.zeros((128, 256), f32), jnp.zeros((8, 128), f32))
    )

    def end_attend():
        def end_keys(d):
            for copy in key_copies(d, x):
                copy.wait_send()

        def end_query(k):
            for copy in query_copies(z - 1 - k, z):
                copy.wait_send()

        def end_result(zq):
            for copy in result_copies(zq, z):
                copy.wait_send()

        loop(1, NX, end_keys)
        loop(0, z, end_query)
        loop(z + 1, nz, end_result)

    ends.append(end_attend)

    def stat_copy(n, d):
        return rcopy(stat.at[n], stats.at[n, d], ss.at[n, d], sr.at[n, d], sp, lax.rem(tp + d, ntp))

    def over_tp(n, rows8):
        stat[n] = rows8
        loop(1, ntp, lambda d: stat_copy(n, d).start())
        ends.append(lambda: loop(1, ntp, lambda d: stat_copy(n, d).wait_send()))
        loop(1, ntp, lambda d: stat_copy(n, d).wait_recv())
        total = rows8
        for d in range(1, ntp):
            total = total + stats[n, d]
        return total

    def halves_of(both):
        left, right = both[:, :128], both[:, 128:]
        return jnp.where(c == 0, left, right), jnp.where(c == 0, right, left)

    halves = ((0, 128), (128, 256))
    misc[...] = jnp.zeros((8, 128), f32)
    misc[0:2, :] = ids_ref[...].astype(f32)
    misc[2:4, :] = route_ref[...]
    facts = misc[...]
    id_cols = spread(facts, (0, 1), halves)
    route_cols = spread(facts, (2, 3), halves)
    lane128 = iota((128, 128), 1)
    lane_f = lane128.astype(f32)
    id_col = (id_cols[:, :128], id_cols[:, 128:])
    hot = [v == lane_f for v in id_col]
    tri = ones_where(iota((128, 128), 0) > lane128)
    earlier = dot(tri, ones_where(hot[0] | hot[1]))
    lane_all = iota((128, nsp * STRIDE), 1).astype(f32)
    choice = []
    for k in range(2):
        slot = jnp.sum(jnp.where(hot[k], earlier, 0.0), axis=1, keepdims=True)
        place = id_col[k][:, :1] * float(STRIDE) + slot
        choice.append(ones_where(place == lane_all))
    row_c, col_c = iota((nsp * CAP, nsp * STRIDE), 0), iota((nsp * CAP, nsp * STRIDE), 1)
    block_c = (row_c * (-(-(1 << 17) // CAP))) >> 17
    compact = ones_where(col_c == row_c + block_c * (STRIDE - CAP))

    squares = over_tp(0, rowsums(attend * attend))
    scale = spread(lax.rsqrt(squares / float(columns) + norm_eps), (0, 4), halves)
    normed_a = (attend[:, :128] * scale[:, :128] * ga_ref[...]).astype(bf16)
    normed_b = (attend[:, 128:] * scale[:, 128:] * gb_ref[...]).astype(bf16)
    loads[0].wait()
    loads[1].wait()

    def project(yy):
        cols = pl.ds(pl.multiple_of(yy * 256, 256), 256)
        return dot(normed_a, pa[:, cols]) + dot(normed_b, pb[:, cols])

    def mate1(d):
        return rcopy(p1s.at[d], p1v.at[d], p1ss.at[d], p1sr.at[d], sp, mate)

    def chip1(d):
        return rcopy(p1r.at[d], p1i.at[d], p1rs.at[d], p1rr.at[d], sp, lax.rem(y + d, ny) * 2 + c)

    def make1(d):
        own, other = halves_of(project(lax.rem(y + d, ny)))
        p1s[d] = other.astype(bf16)
        mate1(d).start()
        p1o[d] = own

    def pass1(d):
        mate1(d).wait_recv()
        p1r[d] = (p1o[d] + p1v[d].astype(f32)).astype(bf16)
        chip1(d).start()

    order = near_order(ny)[::-1]
    make1(order[0])
    for before, d in zip(order, order[1:] + [0]):
        make1(d)
        pass1(before)
    mate1(0).wait_recv()
    mixed = p1o[0] + p1v[0].astype(f32)
    for d in order[::-1]:
        chip1(d).wait_recv()
        mixed = mixed + p1i[d].astype(f32)
    ends.append(lambda: loop(0, ny, lambda d: mate1(d).wait_send()))
    ends.append(lambda: loop(1, ny, lambda d: chip1(d).wait_send()))
    first = depth_scale * res_ref[...].astype(f32) + mixed.astype(bf16).astype(f32)

    def norm(n, total, gain, bias):
        sums = over_tp(n, rowsums(jnp.concatenate([total, total * total], axis=1)))
        mean = sums[0:1, :] / float(columns)
        var = sums[4:5, :] / float(columns) - mean * mean
        wide = spread(jnp.where(row8 < 4, mean, lax.rsqrt(var + norm_eps)), (0, 4), halves)
        return ((total - wide[:, :128]) * wide[:, 128:] * gain + bias).astype(bf16)

    settled = norm(1, first, gs_ref[...], bs_ref[...])

    here = pl.ds(pl.multiple_of(sp * STRIDE, STRIDE), STRIDE)

    def sp_copy(src, dst, send, recv, d):
        peer = lax.rem(sp + d, nsp)
        rows = pl.ds(pl.multiple_of(peer * STRIDE, STRIDE), STRIDE)
        return rcopy(src.at[rows, :], dst.at[here, :], send.at[d], recv.at[d], peer, tp)

    def sp_await(src, dst, send, recv, d):
        peer = lax.rem(sp - d + nsp, nsp)
        rows = pl.ds(pl.multiple_of(peer * STRIDE, STRIDE), STRIDE)
        rcopy(src.at[rows, :], dst.at[rows, :], send.at[d], recv.at[d], peer, tp).wait_recv()

    def exchange(src, dst, send, recv, value):
        src[...] = value
        loop(1, nsp, lambda d: sp_copy(src, dst, send, recv, d).start())
        ends.append(lambda: loop(1, nsp, lambda d: sp_copy(src, dst, send, recv, d).wait_send()))
        dst[here, :] = src[here, :]
        loop(1, nsp, lambda d: sp_await(src, dst, send, recv, d))
        return dst[...]

    arrived = exchange(dsp, drv, ds_, dr_, dot_tl(choice[0] + choice[1], settled).astype(bf16))
    tokens = dot(compact, arrived).astype(bf16)

    half = ny // 2
    height = nsp * CAP // PIECES
    ways = (0, 1)

    def chip_at(steps):
        return lax.rem(y + steps + ny, ny)

    def last_hop(way, p):
        return half if (p < PIECES // 2) == (way == 0) else half - 1

    def block_of(way, hop, core):
        source = chip_at(-hop if way == 0 else hop)
        return source, pl.ds(pl.multiple_of(core * 128, 128), 128)

    def along(way, hop, p):
        source, side = block_of(way, hop, c)
        block = xg.at[source, pl.ds(p * height, height), side]
        target = chip_at(1 if way == 0 else -1) * 2 + c
        return rcopy(block, block, as_.at[way, hop, p], ar_.at[way, hop + 1, p], sp, target)

    def along_await(way, hop, p):
        source, side = block_of(way, hop, c)
        block = xg.at[source, pl.ds(p * height, height), side]
        target = chip_at(-1 if way == 0 else 1) * 2 + c
        rcopy(block, block, as_.at[way, hop, p], ar_.at[way, hop, p], sp, target).wait_recv()

    def across(way, hop, p):
        source, side = block_of(way, hop, c)
        block = xg.at[source, pl.ds(p * height, height), side]
        return rcopy(block, block, hs_.at[way, hop, p], hr_.at[way, hop, p], sp, mate)

    def across_await(way, hop, p):
        source, side = block_of(way, hop, 1 - c)
        block = xg.at[source, pl.ds(p * height, height), side]
        rcopy(block, block, hs_.at[way, hop, p], hr_.at[way, hop, p], sp, mate).wait_recv()

    def take(source, start):
        rows = pl.ds(pl.multiple_of(source * 256, 256), 256)
        block = xg[source]
        gate, up = dot(block, wg[rows, :]), dot(block, wu[rows, :])
        if start:
            acc_g[...] = gate
            acc_u[...] = up
        else:
            acc_g[...] += gate
            acc_u[...] += up

    xg[y, :, pl.ds(pl.multiple_of(c * 128, 128), 128)] = tokens
    sends = [(way, 0, p) for p in range(PIECES) for way in ways if last_hop(way, p) > 0]
    crossings = [(0, 0, p) for p in range(PIECES)]
    for key in sends:
        along(*key).start()
    for key in crossings:
        across(*key).start()
    loads[2].wait()
    loads[3].wait()
    for p in range(PIECES):
        across_await(0, 0, p)
    take(y, True)
    for hop in range(1, half + 1):
        reached = [(way, hop, p) for p in range(PIECES) for way in ways if hop <= last_hop(way, p)]
        for key in reached:
            way, _, p = key
            along_await(*key)
            if hop < last_hop(way, p):
                along(*key).start()
                sends.append(key)
            across(*key).start()
            crossings.append(key)
        for key in reached:
            across_await(*key)
        take(chip_at(-hop), False)
        if hop < half:
            take(chip_at(hop), False)

    def end_gather():
        for key in sends:
            along(*key).wait_send()
        for key in crossings:
            across(*key).wait_send()

    ends.append(end_gather)

    gate = acc_g[...]
    hidden = (gate / (1.0 + jnp.exp(-gate)) * acc_u[...]).astype(bf16)
    loads[4].wait()

    def mate2(d):
        return rcopy(p2s.at[d], p2v.at[d], p2ss.at[d], p2sr.at[d], sp, mate)

    def make2(d):
        cols = pl.ds(pl.multiple_of(lax.rem(y + d, ny) * 256, 256), 256)
        own, other = halves_of(dot(hidden, wd[:, cols]))
        p2s[d] = other.astype(bf16)
        mate2(d).start()
        p2o[d] = own

    def term2(d, p):
        rows = slice(p * height, p * height + height)
        return p2o[d, rows, :] + p2v[d, rows, :].astype(f32)

    def pass2(way, step, p):
        rows = pl.ds(p * height, height)
        target = chip_at(1 if way == 0 else -1) * 2 + c
        return rcopy(
            rb_s.at[way, step, rows, :], rb_r.at[way, step, rows, :],
            rbs_.at[way, step, p], rbr_.at[way, step, p], sp, target,
        )

    passes = []

    def hand_on(step):
        left = half - step
        for p in range(PIECES):
            for way in ways:
                start = half - last_hop(way, p)
                if step < start:
                    continue
                rows = slice(p * height, p * height + height)
                value = term2(left if way == 0 else ny - left, p)
                if step > start:
                    pass2(way, step - 1, p).wait_recv()
                    value = value + rb_r[way, step - 1, rows, :].astype(f32)
                rb_s[way, step, rows, :] = value.astype(bf16)
                pass2(way, step, p).start()
                passes.append((way, step, p))

    make2(half)
    for step in range(half):
        left = half - step
        if left > 1:
            make2(left - 1)
            make2(ny - left + 1)
        else:
            make2(0)
        mate2(left).wait_recv()
        if left < half:
            mate2(ny - left).wait_recv()
        hand_on(step)
    mate2(0).wait_recv()
    outputs = []
    for p in range(PIECES):
        rows = slice(p * height, p * height + height)
        value = term2(0, p)
        for way in ways:
            if last_hop(way, p) > 0:
                pass2(way, half - 1, p).wait_recv()
                value = value + rb_r[way, half - 1, rows, :].astype(f32)
        outputs.append(value.astype(bf16))

    def end_sum():
        loop(0, ny, lambda d: mate2(d).wait_send())
        for key in passes:
            pass2(*key).wait_send()

    ends.append(end_sum)
    outputs = jnp.concatenate(outputs, axis=0)

    returned = exchange(rts, rtv, ts_, tr_, dot_tl(compact, outputs).astype(bf16))
    routed = route_cols[:, :128] * dot(choice[0], returned) + route_cols[:, 128:] * dot(choice[1], returned)
    second = depth_scale * settled.astype(f32) + routed
    out_ref[...] = norm(2, second, gf_ref[...], bf_ref[...])
    for end in ends:
        end()


def body(
    nsp, ntp,
    residual_in, query_alpha, pairs_alpha, offset_alpha, gain_alpha,
    query_beta, pairs_beta, offset_beta, gain_beta, project_alpha, project_beta,
    gain_settle, bias_settle, expert_ids, route_weight,
    expert_gate, expert_up, expert_down, gain_final, bias_final,
):
    nz, ny = nsp // NX, ntp // 2
    vmem = pl.BlockSpec(memory_space=pltpu.VMEM)
    hbm = pl.BlockSpec(memory_space=pl.ANY)
    dma = pltpu.SemaphoreType.DMA
    V = pltpu.VMEM
    rows = nsp * CAP
    wide = nsp * STRIDE
    half = ny // 2
    weights = (project_alpha, project_beta, expert_gate[0], expert_up[0], expert_down[0])
    vectors = [
        v.reshape(1, 128) for v in (gain_alpha, gain_beta, gain_settle, bias_settle, gain_final, bias_final)
    ]
    scratch = [V(w.shape, bf16) for w in weights] + [dma((5,)), V((8, 128), f32)]
    scratch += [
        V((NX * 128, 128), bf16), V((NX * 128, 128), bf16), V((NX * 128, 256), bf16),
        V((8, 128), f32), V((8, NX * 128), f32), V((nz, 128, 128), bf16), V((nz, 128, 128), bf16),
        V((nz, 128, 256), bf16), V((nz, 128, 256), bf16), V((nz, 8, 128), f32), V((nz, 8, 128), f32),
        dma((3, NX)), dma((3, NX)), dma((2, nz)), dma((2, nz)), dma((2, nz)), dma((2, nz)),
    ]
    scratch += [V((3, 8, 128), f32), V((3, ntp, 8, 128), f32), dma((3, ntp)), dma((3, ntp))]
    scratch += [
        V((ny, 128, 128), bf16), V((ny, 128, 128), f32), V((ny, 128, 128), bf16),
        V((ny, 128, 128), bf16), V((ny, 128, 128), bf16), dma((ny,)), dma((ny,)), dma((ny,)), dma((ny,)),
    ]
    scratch += [V((wide, 128), bf16), V((wide, 128), bf16), dma((nsp,)), dma((nsp,))]
    hops = (2, half + 1, PIECES)
    scratch += [
        V((ny, rows, 256), bf16), dma(hops), dma(hops), dma(hops), dma(hops),
        V((rows, expert_gate.shape[2]), f32), V((rows, expert_gate.shape[2]), f32),
    ]
    scratch += [
        V((ny, rows, 128), bf16), V((ny, rows, 128), f32), V((ny, rows, 128), bf16), dma((ny,)), dma((ny,)),
        V((2, half, rows, 128), bf16), V((2, half, rows, 128), bf16), dma(hops), dma(hops),
    ]
    scratch += [V((wide, 128), bf16), V((wide, 128), bf16), dma((nsp,)), dma((nsp,))]
    return pl.pallas_call(
        functools.partial(layer_kernel, nsp, ntp),
        out_shape=jax.ShapeDtypeStruct((128, 128), bf16),
        in_specs=[vmem] * 15 + [hbm] * 5,
        out_specs=vmem,
        scratch_shapes=scratch,
        compiler_params=pltpu.CompilerParams(
            collective_id=0, has_side_effects=True, vmem_limit_bytes=62 * 1024 * 1024
        ),
        name="layer",
    )(
        query_alpha, query_beta, pairs_alpha.reshape(128, 128), pairs_beta.reshape(128, 256),
        offset_alpha.T, offset_beta.T, residual_in, *vectors, expert_ids.T, route_weight.T, *weights,
    )


def solution(mesh):
    in_specs = (
        P("sp", "tp"),
        P("sp", "tp"),
        P("sp", "tp", None),
        P("sp", "tp"),
        P("tp"),
        P("sp", "tp"),
        P("sp", "tp", None),
        P("sp", "tp"),
        P("tp"),
        P("tp", None),
        P("tp", None),
        P("tp"),
        P("tp"),
        P("sp", None),
        P("sp", None),
        P("sp", None, "tp"),
        P("sp", None, "tp"),
        P("sp", "tp", None),
        P("tp"),
        P("tp"),
    )
    step = functools.partial(body, mesh.shape["sp"], mesh.shape["tp"])
    return jax.shard_map(step, mesh=mesh, in_specs=in_specs, out_specs=P("sp", "tp"), check_vma=False)
```

time: 150 us -> 129 us (0.86)
  Pallas kernels: 141 us -> 127 us
  local copies, waits for them, and re-layouts: 7.94 us -> 1.38 us
    pallas_call x1 -> x0, Pallas kernels: 43.7 us -> none  [body(): pl.pallas_call(functools.partial(attend_kernel, nz), out_shape=jax.ShapeD...]
    pallas_call x1, Pallas kernels: 97.7 us -> 127 us  [body(): pl.pallas_call(functools.partial(layer_kernel, nsp, ntp), out_shape=jax.S...]
    unnamed x43 -> x1, local copies, waits for them, and re-layouts: 7.86 us -> 1.38 us
where the time goes in v2:
time: 129 us
  Pallas kernels  127 us (98%)
  local copies, waits for them, and re-layouts  1.38 us (1%)
    pallas_call x1, Pallas kernels, body(): pl.pallas_call(functools.partial(layer_kernel, nsp, ntp), out_shape=jax.S...  127 us

profile of v2, /device:TPU:1, one launch (start us, length us, event | category | flops | bytes accessed | tf_op | source)
XLA Modules:
  0.0 128.7 jit_solution(8650901569139109013)
XLA Ops:
  0.0 127.3 %layer.1 = bf16[128,128]{1,0:T(8,128)(2,1)} custom-call(bf16[128,128]{1,0:T(8,128)(2,1)} %qa_ref.1, bf16[128,128]{1,0:T(8,128)(2,1)} %qb_ref.1, bf16[128,128]{1,0:T(8,128)(2,1)} %bitcast.19, bf16[128,256]{1,0:T(8,128)(2,1)} %bitcast.18, f32[2,128]{1,0:T(2,128)} %bitcast.20, f32[1,128]{1,0:T(1,128)} %bitcast.23, bf16[128,128]{1,0:T(8,128)(2,1)} %res_ref.1, ...), custom_call_target="tpu_custom_call" | custom-call | tf_op jit(solution)/shard_map/layer/pallas_call | solution.py:594
  127.3 1.4 %copy.22 = bf16[128,128]{1,0:T(8,128)(2,1)} copy(bf16[128,128]{1,0:T(8,128)(2,1)} %layer.1) | data formatting | bytes 65536

commit v3 on v2

--- a/solution.py
+++ b/solution.py
@@ -13,6 +13,7 @@
 CAP = 12
 STRIDE = 16
 PIECES = 4
+PLANES = 2
 bf16 = jnp.bfloat16
 f32 = jnp.float32
 
@@ -90,6 +91,7 @@
     pa, pb, wg, wu, wd, wsem, misc,
     kva, kvr, kvb, ofs, off, qba, qbb, ret, back, tot, tback,
     ks, kr, qs, qr, rs, rr,
+    vec, vecs, vs_, vr_, mr, ssp, srv, ds2, dr2,
     stat, stats, ss, sr,
     p1s, p1o, p1v, p1r, p1i, p1ss, p1sr, p1rs, p1rr,
     dsp, drv, ds_, dr_,
@@ -127,16 +129,30 @@
     ofs[...] = jnp.zeros((8, 128), f32)
     ofs[0:2, :] = oa_ref[...]
     ofs[2:3, :] = ob_ref[...]
+    vec[...] = jnp.zeros((8, 128), f32)
+    vec[0:1, :] = gs_ref[...]
+    vec[1:2, :] = bs_ref[...]
     pl.semaphore_wait(barrier, nsp - 1 + ntp - 1)
 
-    def key_copies(d, src_x):
-        peer = z * NX + lax.rem(x + d, NX)
-        rows = pl.ds(pl.multiple_of(src_x * 128, 128), 128)
-        return (
-            rcopy(ka_ref, kva.at[rows, :], ks.at[0, d], kr.at[0, d], peer, tp),
-            rcopy(kb_ref, kvb.at[rows, :], ks.at[1, d], kr.at[1, d], peer, tp),
-            rcopy(ofs, off.at[:, rows], ks.at[2, d], kr.at[2, d], peer, tp),
-        )
+    groups = nz // PLANES
+    zp, zb = lax.div(z, PLANES), lax.rem(z, PLANES)
+    other_z = z + 1 - 2 * zb
+    here_slot, there_slot = zb * NX, (1 - zb) * NX
+
+    def key_copies(passed, k, slot, peer):
+        rows = pl.ds(pl.multiple_of(slot * 128, 128), 128)
+        sources = (kva.at[rows, :], kvb.at[rows, :], off.at[:, rows]) if passed else (ka_ref, kb_ref, ofs)
+        targets = (kva.at[rows, :], kvb.at[rows, :], off.at[:, rows])
+        return [
+            rcopy(src, dst, ks.at[i, k], kr.at[i, k], peer, tp)
+            for i, (src, dst) in enumerate(zip(sources, targets))
+        ]
+
+    def x_peer(d):
+        return z * NX + lax.rem(x + d, NX)
+
+    def cross_copies(slot):
+        return key_copies(False, 0, slot + x, other_z * NX + x)
 
     def query_copies(dst_z, src_z):
         peer = dst_z * NX + x
@@ -152,27 +168,53 @@
             rcopy(tot.at[dst_z], tback.at[src_z], rs.at[1, dst_z], rr.at[1, src_z], peer, tp),
         )
 
+    for copy in cross_copies(here_slot):
+        copy.start()
+
     def send_keys(d):
-        for copy in key_copies(d, x):
+        for copy in key_copies(False, d, here_slot + x, x_peer(d)):
             copy.start()
 
     loop(1, NX, send_keys)
 
     def send_query(k):
-        for copy in query_copies(z - 1 - k, z):
+        for copy in query_copies(z - PLANES * (k + 1), z):
             copy.start()
 
-    loop(0, z, send_query)
-
-    mine = pl.ds(pl.multiple_of(x * 128, 128), 128)
+    loop(0, zp, send_query)
+
+    def vec_copy(d):
+        return rcopy(vec, vecs.at[tp], vs_.at[d], vr_.at[d], sp, lax.rem(tp + d, ntp))
+
+    def vec_await(d):
+        source = lax.rem(tp - d + ntp, ntp)
+        rcopy(vec, vecs.at[source], vs_.at[d], vr_.at[d], sp, source).wait_recv()
+
+    loop(1, ntp, lambda d: vec_copy(d).start())
+    ends.append(lambda: loop(1, ntp, lambda d: vec_copy(d).wait_send()))
+    vecs[tp] = vec[...]
+
+    mine = pl.ds(pl.multiple_of((here_slot + x) * 128, 128), 128)
     kva[mine, :] = ka_ref[...]
     kvb[mine, :] = kb_ref[...]
     off[:, mine] = ofs[...]
     qba[z] = qa_ref[...]
     qbb[z] = qb_ref[...]
 
+    for copy in cross_copies(there_slot):
+        copy.wait_recv()
+
+    def pass_keys(d):
+        for copy in key_copies(True, NX + d, there_slot + x, x_peer(d)):
+            copy.start()
+
+    loop(1, NX, pass_keys)
+
     def await_keys(d):
-        for copy in key_copies(d, lax.rem(x - d + NX, NX)):
+        source = lax.rem(x - d + NX, NX)
+        for copy in key_copies(False, d, here_slot + source, x_peer(d)):
+            copy.wait_recv()
+        for copy in key_copies(True, NX + d, there_slot + source, x_peer(d)):
             copy.wait_recv()
 
     loop(1, NX, await_keys)
@@ -183,10 +225,12 @@
     gap = lane - iota((128, 128), 0)
     r256, c256 = iota((256, 256), 0) & 127, iota((256, 256), 1)
     later_matrix = ones_where((r256 > c256) | (c256 >= 128))
-    ones8 = jnp.ones((8, 256), bf16)
+    first_lane = ones_where((iota((8, 384), 1) & 127) == 0)
     row8 = iota((8, 128), 0)
 
-    def visit(zq):
+    def visit(m):
+        zq = z + PLANES * m
+
         @pl.when(zq > z)
         def _():
             for copy in query_copies(z, zq):
@@ -199,23 +243,21 @@
             q = (jnp.where(lane < 64, qa, zero), jnp.where(lane >= 64, qa, zero), qb)[h]
             scale = (64.0**-0.5, 64.0**-0.5, 128.0**-0.5)[h]
             gone = jnp.zeros((128, 128), f32)
-            total = jnp.zeros((8, 128), f32)
-            weights = [None] * NX
-            for b in reversed(range(NX)):
+            weights = [None] * (PLANES * NX)
+            for b in reversed(range(PLANES * NX)):
                 rows = slice(b * 128, b * 128 + 128)
                 keys = (kva[rows, :], kvr[rows, :], kvb[rows, :128])[h]
                 scores = dot_tr(q, keys) * scale + off[h : h + 1, rows]
-                valid = gap < (zq - z) * (NX * 128) + (x - b) * 128
+                valid = gap < ((zq - zp * PLANES) * NX + x - b) * 128
                 soft = jnp.maximum(scores, 0.0) + jnp.log(1.0 + jnp.exp(-jnp.abs(scores)))
                 cat = jnp.concatenate(split(jnp.where(valid, soft, 0.0), 2), axis=1)
                 sums = dot(cat, later_matrix)
-                total = total + dot_tr(ones8, cat)
                 power = (scores - soft) - (sums[:, :128] + gone)
                 gone = gone + sums[:, 128:]
                 weights[b] = jnp.where(valid, jnp.exp(power), 0.0).astype(bf16)
             values = (kvr[...], kva[...], kvb[:, 128:])[h]
             accs.append(dot(jnp.concatenate(weights, axis=1), values))
-            totals.append(total)
+            totals.append(dot_tr(first_lane, jnp.concatenate(split(gone, 3), axis=1)))
         both = jnp.where(lane < 64, accs[0], accs[1])
         found = jnp.concatenate([both, accs[2]], axis=1).astype(bf16)
         sums8 = jnp.where(row8 == 0, totals[0], jnp.where(row8 == 1, totals[1], totals[2]))
@@ -232,11 +274,11 @@
             for copy in result_copies(zq, z):
                 copy.start()
 
-    loop(z, nz, visit)
+    loop(0, groups - zp, visit)
 
     def gather(k, carry):
         acc, gone = carry
-        zk = z - k
+        zk = z - PLANES * k
 
         @pl.when(k > 0)
         def _():
@@ -247,35 +289,42 @@
         return acc + wide * back[zk].astype(f32), gone + tback[zk]
 
     attend, _ = lax.fori_loop(
-        0, z + 1, gather, (jnp.zeros((128, 256), f32), jnp.zeros((8, 128), f32))
+        0, zp + 1, gather, (jnp.zeros((128, 256), f32), jnp.zeros((8, 128), f32))
     )
 
     def end_attend():
+        for copy in cross_copies(here_slot):
+            copy.wait_send()
+
         def end_keys(d):
-            for copy in key_copies(d, x):
+            for copy in key_copies(False, d, here_slot + x, x_peer(d)):
                 copy.wait_send()
+            for copy in key_copies(True, NX + d, there_slot + x, x_peer(d)):
+                copy.wait_send()
 
         def end_query(k):
-            for copy in query_copies(z - 1 - k, z):
+            for copy in query_copies(z - PLANES * (k + 1), z):
                 copy.wait_send()
 
-        def end_result(zq):
-            for copy in result_copies(zq, z):
+        def end_result(m):
+            for copy in result_copies(z + PLANES * m, z):
                 copy.wait_send()
 
         loop(1, NX, end_keys)
-        loop(0, z, end_query)
-        loop(z + 1, nz, end_result)
+        loop(0, zp, end_query)
+        loop(1, groups - zp, end_result)
 
     ends.append(end_attend)
 
     def stat_copy(n, d):
         return rcopy(stat.at[n], stats.at[n, d], ss.at[n, d], sr.at[n, d], sp, lax.rem(tp + d, ntp))
 
-    def over_tp(n, rows8):
+    def begin_tp(n, rows8):
         stat[n] = rows8
         loop(1, ntp, lambda d: stat_copy(n, d).start())
         ends.append(lambda: loop(1, ntp, lambda d: stat_copy(n, d).wait_send()))
+
+    def finish_tp(n, rows8):
         loop(1, ntp, lambda d: stat_copy(n, d).wait_recv())
         total = rows8
         for d in range(1, ntp):
@@ -309,7 +358,9 @@
     block_c = (row_c * (-(-(1 << 17) // CAP))) >> 17
     compact = ones_where(col_c == row_c + block_c * (STRIDE - CAP))
 
-    squares = over_tp(0, rowsums(attend * attend))
+    own_squares = rowsums(attend * attend)
+    begin_tp(0, own_squares)
+    squares = finish_tp(0, own_squares)
     scale = spread(lax.rsqrt(squares / float(columns) + norm_eps), (0, 4), halves)
     normed_a = (attend[:, :128] * scale[:, :128] * ga_ref[...]).astype(bf16)
     normed_b = (attend[:, 128:] * scale[:, 128:] * gb_ref[...]).astype(bf16)
@@ -351,14 +402,21 @@
     ends.append(lambda: loop(1, ny, lambda d: chip1(d).wait_send()))
     first = depth_scale * res_ref[...].astype(f32) + mixed.astype(bf16).astype(f32)
 
-    def norm(n, total, gain, bias):
-        sums = over_tp(n, rowsums(jnp.concatenate([total, total * total], axis=1)))
+    def begin_norm(n, total):
+        sums = rowsums(jnp.concatenate([total, total * total], axis=1))
+        begin_tp(n, sums)
+        return sums
+
+    def moments(n, sums):
+        sums = finish_tp(n, sums)
         mean = sums[0:1, :] / float(columns)
         var = sums[4:5, :] / float(columns) - mean * mean
-        wide = spread(jnp.where(row8 < 4, mean, lax.rsqrt(var + norm_eps)), (0, 4), halves)
+        return spread(jnp.where(row8 < 4, mean, lax.rsqrt(var + norm_eps)), (0, 4), halves)
+
+    def normed(total, wide, gain, bias):
         return ((total - wide[:, :128]) * wide[:, 128:] * gain + bias).astype(bf16)
 
-    settled = norm(1, first, gs_ref[...], bs_ref[...])
+    own_sums = begin_norm(1, first)
 
     here = pl.ds(pl.multiple_of(sp * STRIDE, STRIDE), STRIDE)
 
@@ -372,16 +430,26 @@
         rows = pl.ds(pl.multiple_of(peer * STRIDE, STRIDE), STRIDE)
         rcopy(src.at[rows, :], dst.at[rows, :], send.at[d], recv.at[d], peer, tp).wait_recv()
 
-    def exchange(src, dst, send, recv, value):
+    def post(src, dst, send, recv, value):
         src[...] = value
         loop(1, nsp, lambda d: sp_copy(src, dst, send, recv, d).start())
         ends.append(lambda: loop(1, nsp, lambda d: sp_copy(src, dst, send, recv, d).wait_send()))
         dst[here, :] = src[here, :]
+
+    def collect(src, dst, send, recv):
         loop(1, nsp, lambda d: sp_await(src, dst, send, recv, d))
         return dst[...]
 
-    arrived = exchange(dsp, drv, ds_, dr_, dot_tl(choice[0] + choice[1], settled).astype(bf16))
-    tokens = dot(compact, arrived).astype(bf16)
+    routes = choice[0] + choice[1]
+    post(dsp, drv, ds_, dr_, dot_tl(routes, first.astype(bf16)).astype(bf16))
+    wide = moments(1, own_sums)
+    pieces = split(wide[:, :128], 3) + split(wide[:, 128:], 3)
+    packed = jnp.zeros((128, 128), f32)
+    for i, piece in enumerate(pieces):
+        packed = jnp.where(lane128 == i, piece.astype(f32), packed)
+    post(ssp, srv, ds2, dr2, dot_tl(routes, packed.astype(bf16)).astype(bf16))
+    settled = normed(first, wide, gs_ref[...], bs_ref[...])
+    tokens = dot(compact, collect(dsp, drv, ds_, dr_)).astype(bf16)
 
     half = ny // 2
     height = nsp * CAP // PIECES
@@ -421,7 +489,13 @@
 
     def take(source, start):
         rows = pl.ds(pl.multiple_of(source * 256, 256), 256)
-        block = xg[source]
+        block = xg[source].astype(f32)
+        mean, factor = mr[:, :128], mr[:, 128:]
+        sides = []
+        for i in range(2):
+            gain, bias = vecs[source * 2 + i, 0:1, :], vecs[source * 2 + i, 1:2, :]
+            sides.append((block[:, i * 128 : i * 128 + 128] - mean) * factor * gain + bias)
+        block = jnp.concatenate(sides, axis=1).astype(bf16)
         gate, up = dot(block, wg[rows, :]), dot(block, wu[rows, :])
         if start:
             acc_g[...] = gate
@@ -439,6 +513,11 @@
         across(*key).start()
     loads[2].wait()
     loads[3].wait()
+    loop(1, ntp, vec_await)
+    row_m, col_m = iota((128, 256), 0), iota((128, 256), 1)
+    unpack = ones_where(((row_m < 3) & (col_m < 128)) | ((row_m >= 3) & (row_m < 6) & (col_m >= 128)))
+    numbers = dot(compact, collect(ssp, srv, ds2, dr2)).astype(bf16)
+    mr[...] = dot(numbers, unpack)
     for p in range(PIECES):
         across_await(0, 0, p)
     take(y, True)
@@ -541,10 +620,12 @@
     ends.append(end_sum)
     outputs = jnp.concatenate(outputs, axis=0)
 
-    returned = exchange(rts, rtv, ts_, tr_, dot_tl(compact, outputs).astype(bf16))
+    post(rts, rtv, ts_, tr_, dot_tl(compact, outputs).astype(bf16))
+    returned = collect(rts, rtv, ts_, tr_)
     routed = route_cols[:, :128] * dot(choice[0], returned) + route_cols[:, 128:] * dot(choice[1], returned)
     second = depth_scale * settled.astype(f32) + routed
-    out_ref[...] = norm(2, second, gf_ref[...], bf_ref[...])
+    last_sums = begin_norm(2, second)
+    out_ref[...] = normed(second, moments(2, last_sums), gf_ref[...], bf_ref[...])
     for end in ends:
         end()
 
@@ -563,6 +644,7 @@
     V = pltpu.VMEM
     rows = nsp * CAP
     wide = nsp * STRIDE
+    keys = PLANES * NX * 128
     half = ny // 2
     weights = (project_alpha, project_beta, expert_gate[0], expert_up[0], expert_down[0])
     vectors = [
@@ -570,10 +652,14 @@
     ]
     scratch = [V(w.shape, bf16) for w in weights] + [dma((5,)), V((8, 128), f32)]
     scratch += [
-        V((NX * 128, 128), bf16), V((NX * 128, 128), bf16), V((NX * 128, 256), bf16),
-        V((8, 128), f32), V((8, NX * 128), f32), V((nz, 128, 128), bf16), V((nz, 128, 128), bf16),
+        V((keys, 128), bf16), V((keys, 128), bf16), V((keys, 256), bf16),
+        V((8, 128), f32), V((8, keys), f32), V((nz, 128, 128), bf16), V((nz, 128, 128), bf16),
         V((nz, 128, 256), bf16), V((nz, 128, 256), bf16), V((nz, 8, 128), f32), V((nz, 8, 128), f32),
-        dma((3, NX)), dma((3, NX)), dma((2, nz)), dma((2, nz)), dma((2, nz)), dma((2, nz)),
+        dma((3, 2 * NX)), dma((3, 2 * NX)), dma((2, nz)), dma((2, nz)), dma((2, nz)), dma((2, nz)),
+    ]
+    scratch += [
+        V((8, 128), f32), V((ntp, 8, 128), f32), dma((ntp,)), dma((ntp,)), V((rows, 256), f32),
+        V((wide, 128), bf16), V((wide, 128), bf16), dma((nsp,)), dma((nsp,)),
     ]
     scratch += [V((3, 8, 128), f32), V((3, ntp, 8, 128), f32), dma((3, ntp)), dma((3, ntp))]
     scratch += [

time: 129 us -> 121 us (0.938)
  Pallas kernels: 127 us -> 120 us
    pallas_call x1, Pallas kernels: 127 us -> 120 us  [body(): pl.pallas_call(functools.partial(layer_kernel, nsp, ntp), out_shape=jax.S...]
where the time goes in v3:
time: 121 us
  Pallas kernels  120 us (99%)
  local copies, waits for them, and re-layouts  1.38 us (1%)
    pallas_call x1, Pallas kernels, body(): pl.pallas_call(functools.partial(layer_kernel, nsp, ntp), out_shape=jax.S...  120 us

profile of v3, /device:TPU:1, one launch (start us, length us, event | category | flops | bytes accessed | tf_op | source)
XLA Modules:
  0.0 120.9 jit_solution(4195155843921294629)
XLA Ops:
  0.0 119.5 %layer.1 = bf16[128,128]{1,0:T(8,128)(2,1)} custom-call(bf16[128,128]{1,0:T(8,128)(2,1)} %qa_ref.1, bf16[128,128]{1,0:T(8,128)(2,1)} %qb_ref.1, bf16[128,128]{1,0:T(8,128)(2,1)} %bitcast.19, bf16[128,256]{1,0:T(8,128)(2,1)} %bitcast.18, f32[2,128]{1,0:T(2,128)} %bitcast.20, f32[1,128]{1,0:T(1,128)} %bitcast.23, bf16[128,128]{1,0:T(8,128)(2,1)} %res_ref.1, ...), custom_call_target="tpu_custom_call" | custom-call | tf_op jit(solution)/shard_map/layer/pallas_call | solution.py:680
  119.6 1.4 %copy.22 = bf16[128,128]{1,0:T(8,128)(2,1)} copy(bf16[128,128]{1,0:T(8,128)(2,1)} %layer.1) | data formatting | bytes 65536

commit v4 on v3

--- a/solution.py
+++ b/solution.py
@@ -88,7 +88,7 @@
     nsp, ntp,
     qa_ref, qb_ref, ka_ref, kb_ref, oa_ref, ob_ref, res_ref, ga_ref, gb_ref, gs_ref, bs_ref, gf_ref, bf_ref,
     ids_ref, route_ref, pa_hbm, pb_hbm, wg_hbm, wu_hbm, wd_hbm, out_ref,
-    pa, pb, wg, wu, wd, wsem, misc,
+    held, hsem, pa, pb, wg, wu, wd, wsem, misc,
     kva, kvr, kvb, ofs, off, qba, qbb, ret, back, tot, tback,
     ks, kr, qs, qr, rs, rr,
     vec, vecs, vs_, vr_, mr, ssp, srv, ds2, dr2,
@@ -113,19 +113,32 @@
             ((pa_hbm, pa), (pb_hbm, pb), (wg_hbm, wg), (wu_hbm, wu), (wd_hbm, wd))
         )
     ]
+    given = (
+        qa_ref, qb_ref, ka_ref, kb_ref, oa_ref, ob_ref, res_ref,
+        ga_ref, gb_ref, gs_ref, bs_ref, gf_ref, bf_ref, ids_ref, route_ref,
+    )
+    fetches = [pltpu.make_async_copy(src, dst, hsem.at[i]) for i, (src, dst) in enumerate(zip(given, held))]
+    for load in fetches:
+        load.start()
+    (
+        qa_ref, qb_ref, ka_ref, kb_ref, oa_ref, ob_ref, res_ref,
+        ga_ref, gb_ref, gs_ref, bs_ref, gf_ref, bf_ref, ids_ref, route_ref,
+    ) = held
+
+    barrier = pltpu.get_barrier_semaphore()
+
+    def greet_sp(d):
+        pl.semaphore_signal(barrier, 1, device_id=(lax.rem(sp + d, nsp), tp), device_id_type=MESH)
+
+    def greet_tp(d):
+        pl.semaphore_signal(barrier, 1, device_id=(sp, lax.rem(tp + d, ntp)), device_id_type=MESH)
+
+    loop(1, nsp, greet_sp)
+    loop(1, ntp, greet_tp)
+    for load in fetches:
+        load.wait()
     for load in loads:
         load.start()
-
-    barrier = pltpu.get_barrier_semaphore()
-
-    def greet_sp(d):
-        pl.semaphore_signal(barrier, 1, device_id=(lax.rem(sp + d, nsp), tp), device_id_type=MESH)
-
-    def greet_tp(d):
-        pl.semaphore_signal(barrier, 1, device_id=(sp, lax.rem(tp + d, ntp)), device_id_type=MESH)
-
-    loop(1, nsp, greet_sp)
-    loop(1, ntp, greet_tp)
     ofs[...] = jnp.zeros((8, 128), f32)
     ofs[0:2, :] = oa_ref[...]
     ofs[2:3, :] = ob_ref[...]
@@ -360,41 +373,42 @@
 
     own_squares = rowsums(attend * attend)
     begin_tp(0, own_squares)
+    gained_a = (attend[:, :128] * ga_ref[...]).astype(bf16)
+    gained_b = (attend[:, 128:] * gb_ref[...]).astype(bf16)
+    loads[0].wait()
+    loads[1].wait()
+
+    def project(yy):
+        cols = pl.ds(pl.multiple_of(yy * 256, 256), 256)
+        return halves_of(dot(gained_a, pa[:, cols])), halves_of(dot(gained_b, pb[:, cols]))
+
+    def mate1(d):
+        return rcopy(p1s.at[d], p1v.at[d], p1ss.at[d], p1sr.at[d], sp, mate)
+
+    def chip1(d):
+        return rcopy(p1r.at[d], p1i.at[d], p1rs.at[d], p1rr.at[d], sp, lax.rem(y + d, ny) * 2 + c)
+
+    def make1(d):
+        (own_a, other_a), (own_b, other_b) = project(lax.rem(y + d, ny))
+        p1s[d] = jnp.concatenate([other_a, other_b], axis=1).astype(bf16)
+        mate1(d).start()
+        p1o[d] = jnp.concatenate([own_a, own_b], axis=1)
+
+    order = near_order(ny)[::-1]
+    for d in order + [0]:
+        make1(d)
     squares = finish_tp(0, own_squares)
     scale = spread(lax.rsqrt(squares / float(columns) + norm_eps), (0, 4), halves)
-    normed_a = (attend[:, :128] * scale[:, :128] * ga_ref[...]).astype(bf16)
-    normed_b = (attend[:, 128:] * scale[:, 128:] * gb_ref[...]).astype(bf16)
-    loads[0].wait()
-    loads[1].wait()
-
-    def project(yy):
-        cols = pl.ds(pl.multiple_of(yy * 256, 256), 256)
-        return dot(normed_a, pa[:, cols]) + dot(normed_b, pb[:, cols])
-
-    def mate1(d):
-        return rcopy(p1s.at[d], p1v.at[d], p1ss.at[d], p1sr.at[d], sp, mate)
-
-    def chip1(d):
-        return rcopy(p1r.at[d], p1i.at[d], p1rs.at[d], p1rr.at[d], sp, lax.rem(y + d, ny) * 2 + c)
-
-    def make1(d):
-        own, other = halves_of(project(lax.rem(y + d, ny)))
-        p1s[d] = other.astype(bf16)
-        mate1(d).start()
-        p1o[d] = own
-
-    def pass1(d):
+
+    def chip_sum(d):
         mate1(d).wait_recv()
-        p1r[d] = (p1o[d] + p1v[d].astype(f32)).astype(bf16)
+        both = (p1o[d] + p1v[d].astype(f32)) * scale
+        return both[:, :128] + both[:, 128:]
+
+    for d in order:
+        p1r[d] = chip_sum(d).astype(bf16)
         chip1(d).start()
-
-    order = near_order(ny)[::-1]
-    make1(order[0])
-    for before, d in zip(order, order[1:] + [0]):
-        make1(d)
-        pass1(before)
-    mate1(0).wait_recv()
-    mixed = p1o[0] + p1v[0].astype(f32)
+    mixed = chip_sum(0)
     for d in order[::-1]:
         chip1(d).wait_recv()
         mixed = mixed + p1i[d].astype(f32)
@@ -511,17 +525,7 @@
         along(*key).start()
     for key in crossings:
         across(*key).start()
-    loads[2].wait()
-    loads[3].wait()
-    loop(1, ntp, vec_await)
-    row_m, col_m = iota((128, 256), 0), iota((128, 256), 1)
-    unpack = ones_where(((row_m < 3) & (col_m < 128)) | ((row_m >= 3) & (row_m < 6) & (col_m >= 128)))
-    numbers = dot(compact, collect(ssp, srv, ds2, dr2)).astype(bf16)
-    mr[...] = dot(numbers, unpack)
-    for p in range(PIECES):
-        across_await(0, 0, p)
-    take(y, True)
-    for hop in range(1, half + 1):
+    def advance(hop):
         reached = [(way, hop, p) for p in range(PIECES) for way in ways if hop <= last_hop(way, p)]
         for key in reached:
             way, _, p = key
@@ -531,11 +535,30 @@
                 sends.append(key)
             across(*key).start()
             crossings.append(key)
+        return reached
+
+    def consume(hop, reached):
         for key in reached:
             across_await(*key)
-        take(chip_at(-hop), False)
+        take(chip_at(-hop), hop == 0)
+        if 0 < hop < half:
+            take(chip_at(hop), False)
+
+    before = list(crossings)
+    following = advance(1)
+    loads[2].wait()
+    loads[3].wait()
+    loop(1, ntp, vec_await)
+    row_m, col_m = iota((128, 256), 0), iota((128, 256), 1)
+    unpack = ones_where(((row_m < 3) & (col_m < 128)) | ((row_m >= 3) & (row_m < 6) & (col_m >= 128)))
+    numbers = dot(compact, collect(ssp, srv, ds2, dr2)).astype(bf16)
+    mr[...] = dot(numbers, unpack)
+    consume(0, before)
+    for hop in range(1, half + 1):
+        before = following
         if hop < half:
-            take(chip_at(hop), False)
+            following = advance(hop + 1)
+        consume(hop, before)
 
     def end_gather():
         for key in sends:
@@ -650,7 +673,12 @@
     vectors = [
         v.reshape(1, 128) for v in (gain_alpha, gain_beta, gain_settle, bias_settle, gain_final, bias_final)
     ]
-    scratch = [V(w.shape, bf16) for w in weights] + [dma((5,)), V((8, 128), f32)]
+    inputs = (
+        query_alpha, query_beta, pairs_alpha.reshape(128, 128), pairs_beta.reshape(128, 256),
+        offset_alpha.T, offset_beta.T, residual_in, *vectors, expert_ids.T, route_weight.T,
+    )
+    scratch = [tuple(V(a.shape, a.dtype) for a in inputs), dma((len(inputs),))]
+    scratch += [V(w.shape, bf16) for w in weights] + [dma((5,)), V((8, 128), f32)]
     scratch += [
         V((keys, 128), bf16), V((keys, 128), bf16), V((keys, 256), bf16),
         V((8, 128), f32), V((8, keys), f32), V((nz, 128, 128), bf16), V((nz, 128, 128), bf16),
@@ -663,7 +691,7 @@
     ]
     scratch += [V((3, 8, 128), f32), V((3, ntp, 8, 128), f32), dma((3, ntp)), dma((3, ntp))]
     scratch += [
-        V((ny, 128, 128), bf16), V((ny, 128, 128), f32), V((ny, 128, 128), bf16),
+        V((ny, 128, 256), bf16), V((ny, 128, 256), f32), V((ny, 128, 256), bf16),
         V((ny, 128, 128), bf16), V((ny, 128, 128), bf16), dma((ny,)), dma((ny,)), dma((ny,)), dma((ny,)),
     ]
     scratch += [V((wide, 128), bf16), V((wide, 128), bf16), dma((nsp,)), dma((nsp,))]
@@ -680,17 +708,14 @@
     return pl.pallas_call(
         functools.partial(layer_kernel, nsp, ntp),
         out_shape=jax.ShapeDtypeStruct((128, 128), bf16),
-        in_specs=[vmem] * 15 + [hbm] * 5,
+        in_specs=[hbm] * 20,
         out_specs=vmem,
         scratch_shapes=scratch,
         compiler_params=pltpu.CompilerParams(
             collective_id=0, has_side_effects=True, vmem_limit_bytes=62 * 1024 * 1024
         ),
         name="layer",
-    )(
-        query_alpha, query_beta, pairs_alpha.reshape(128, 128), pairs_beta.reshape(128, 256),
-        offset_alpha.T, offset_beta.T, residual_in, *vectors, expert_ids.T, route_weight.T, *weights,
-    )
+    )(*inputs, *weights)
 
 
 def solution(mesh):

time: 121 us -> 118 us (0.975)
  Pallas kernels: 120 us -> 116 us
    pallas_call x1, Pallas kernels: 120 us -> 116 us  [body(): pl.pallas_call(functools.partial(layer_kernel, nsp, ntp), out_shape=jax.S...]
where the time goes in v4:
time: 118 us; the launch traced here: 117 us
  Pallas kernels  116 us (98%)
  local copies, waits for them, and re-layouts  1.38 us (1%)
    pallas_call x1, Pallas kernels, body(): pl.pallas_call(functools.partial(layer_kernel, nsp, ntp), out_shape=jax.S...  116 us

profile of v4, /device:TPU:1, one launch (start us, length us, event | category | flops | bytes accessed | tf_op | source)
XLA Modules:
  0.0 117.4 jit_solution(14116146800077544514)
XLA Ops:
  0.0 116.0 %layer.1 = bf16[128,128]{1,0:T(8,128)(2,1)} custom-call(bf16[128,128]{1,0:T(8,128)(2,1)} %qa_ref.1, bf16[128,128]{1,0:T(8,128)(2,1)} %qb_ref.1, bf16[128,128]{1,0:T(8,128)(2,1)} %bitcast.19, bf16[128,256]{1,0:T(8,128)(2,1)} %bitcast.18, f32[2,128]{1,0:T(2,128)} %bitcast.20, f32[1,128]{1,0:T(1,128)} %bitcast.23, bf16[128,128]{1,0:T(8,128)(2,1)} %res_ref.1, ...), custom_call_target="tpu_custom_call" | custom-call | tf_op jit(solution)/shard_map/layer/pallas_call | solution.py:708
  116.1 1.4 %copy.22 = bf16[128,128]{1,0:T(8,128)(2,1)} copy(bf16[128,128]{1,0:T(8,128)(2,1)} %layer.1) | data formatting | bytes 65536

commit v5 on v4

--- a/solution.py
+++ b/solution.py
@@ -241,33 +241,32 @@
     first_lane = ones_where((iota((8, 384), 1) & 127) == 0)
     row8 = iota((8, 128), 0)
 
-    def visit(m):
+    def visit(m, own):
         zq = z + PLANES * m
-
-        @pl.when(zq > z)
-        def _():
+        if not own:
             for copy in query_copies(z, zq):
                 copy.wait_recv()
 
-        qa, qb = qba[zq], qbb[zq]
+        qa, qb = (qba[zq].astype(f32) * 64.0**-0.5).astype(bf16), qbb[zq]
         zero = jnp.zeros_like(qa)
         accs, totals = [], []
         for h in range(3):
             q = (jnp.where(lane < 64, qa, zero), jnp.where(lane >= 64, qa, zero), qb)[h]
-            scale = (64.0**-0.5, 64.0**-0.5, 128.0**-0.5)[h]
             gone = jnp.zeros((128, 128), f32)
             weights = [None] * (PLANES * NX)
             for b in reversed(range(PLANES * NX)):
                 rows = slice(b * 128, b * 128 + 128)
                 keys = (kva[rows, :], kvr[rows, :], kvb[rows, :128])[h]
-                scores = dot_tr(q, keys) * scale + off[h : h + 1, rows]
+                scores = dot_tr(q, keys)
+                scores = (scores * 128.0**-0.5 if h == 2 else scores) + off[h : h + 1, rows]
                 valid = gap < ((zq - zp * PLANES) * NX + x - b) * 128
                 soft = jnp.maximum(scores, 0.0) + jnp.log(1.0 + jnp.exp(-jnp.abs(scores)))
-                cat = jnp.concatenate(split(jnp.where(valid, soft, 0.0), 2), axis=1)
+                cat = jnp.concatenate(split(jnp.where(valid, soft, 0.0) if own else soft, 2), axis=1)
                 sums = dot(cat, later_matrix)
                 power = (scores - soft) - (sums[:, :128] + gone)
                 gone = gone + sums[:, 128:]
-                weights[b] = jnp.where(valid, jnp.exp(power), 0.0).astype(bf16)
+                weight = jnp.exp(power)
+                weights[b] = (jnp.where(valid, weight, 0.0) if own else weight).astype(bf16)
             values = (kvr[...], kva[...], kvb[:, 128:])[h]
             accs.append(dot(jnp.concatenate(weights, axis=1), values))
             totals.append(dot_tr(first_lane, jnp.concatenate(split(gone, 3), axis=1)))
@@ -275,19 +274,17 @@
         found = jnp.concatenate([both, accs[2]], axis=1).astype(bf16)
         sums8 = jnp.where(row8 == 0, totals[0], jnp.where(row8 == 1, totals[1], totals[2]))
 
-        @pl.when(zq == z)
-        def _():
+        if own:
             back[z] = found
             tback[z] = sums8
-
-        @pl.when(zq > z)
-        def _():
+        else:
             ret[zq] = found
             tot[zq] = sums8
             for copy in result_copies(zq, z):
                 copy.start()
 
-    loop(0, groups - zp, visit)
+    visit(0, True)
+    loop(1, groups - zp, lambda m: visit(m, False))
 
     def gather(k, carry):
         acc, gone = carry
@@ -648,9 +645,10 @@
     routed = route_cols[:, :128] * dot(choice[0], returned) + route_cols[:, 128:] * dot(choice[1], returned)
     second = depth_scale * settled.astype(f32) + routed
     last_sums = begin_norm(2, second)
+    for end in ends[:-1]:
+        end()
     out_ref[...] = normed(second, moments(2, last_sums), gf_ref[...], bf_ref[...])
-    for end in ends:
-        end()
+    ends[-1]()
 
 
 def body(

time: 118 us -> 116 us (0.983)
  Pallas kernels: 116 us -> 114 us
    pallas_call x1, Pallas kernels: 116 us -> 114 us  [body(): pl.pallas_call(functools.partial(layer_kernel, nsp, ntp), out_shape=jax.S...]
where the time goes in v5:
time: 116 us; the launch traced here: 115 us
  Pallas kernels  114 us (98%)
  local copies, waits for them, and re-layouts  1.38 us (1%)
    pallas_call x1, Pallas kernels, body(): pl.pallas_call(functools.partial(layer_kernel, nsp, ntp), out_shape=jax.S...  114 us

profile of v5, /device:TPU:1, one launch (start us, length us, event | category | flops | bytes accessed | tf_op | source)
XLA Modules:
  0.0 115.4 jit_solution(17586364970613227285)
XLA Ops:
  0.0 114.0 %layer.1 = bf16[128,128]{1,0:T(8,128)(2,1)} custom-call(bf16[128,128]{1,0:T(8,128)(2,1)} %qa_ref.1, bf16[128,128]{1,0:T(8,128)(2,1)} %qb_ref.1, bf16[128,128]{1,0:T(8,128)(2,1)} %bitcast.19, bf16[128,256]{1,0:T(8,128)(2,1)} %bitcast.18, f32[2,128]{1,0:T(2,128)} %bitcast.20, f32[1,128]{1,0:T(1,128)} %bitcast.23, bf16[128,128]{1,0:T(8,128)(2,1)} %res_ref.1, ...), custom_call_target="tpu_custom_call" | custom-call | tf_op jit(solution)/shard_map/layer/pallas_call | solution.py:706
  114.1 1.4 %copy.22 = bf16[128,128]{1,0:T(8,128)(2,1)} copy(bf16[128,128]{1,0:T(8,128)(2,1)} %layer.1) | data formatting | bytes 65536

commit v6 on v5

--- a/solution.py
+++ b/solution.py
@@ -90,7 +90,7 @@
     ids_ref, route_ref, pa_hbm, pb_hbm, wg_hbm, wu_hbm, wd_hbm, out_ref,
     held, hsem, pa, pb, wg, wu, wd, wsem, misc,
     kva, kvr, kvb, ofs, off, qba, qbb, ret, back, tot, tback,
-    ks, kr, qs, qr, rs, rr,
+    ks, kr, qs, qr, rs, rr, own_acc, own_gone,
     vec, vecs, vs_, vr_, mr, ssp, srv, ds2, dr2,
     stat, stats, ss, sr,
     p1s, p1o, p1v, p1r, p1i, p1ss, p1sr, p1rs, p1rr,
@@ -224,15 +224,19 @@
     loop(1, NX, pass_keys)
 
     def await_keys(d):
-        source = lax.rem(x - d + NX, NX)
-        for copy in key_copies(False, d, here_slot + source, x_peer(d)):
+        for copy in key_copies(False, d, here_slot + lax.rem(x - d + NX, NX), x_peer(d)):
             copy.wait_recv()
-        for copy in key_copies(True, NX + d, there_slot + source, x_peer(d)):
+
+    def await_passed(d):
+        for copy in key_copies(True, NX + d, there_slot + lax.rem(x - d + NX, NX), x_peer(d)):
             copy.wait_recv()
 
-    loop(1, NX, await_keys)
-    keys_a = kva[...]
-    kvr[...] = pltpu.roll(keys_a.astype(f32), 64, 1).astype(bf16)
+    def plane_rows(slot, b, blocks):
+        return pl.ds(pl.multiple_of((slot + b) * 128, 128), blocks * 128)
+
+    def swap_sides(slot):
+        rows = plane_rows(slot, 0, NX)
+        kvr[rows, :] = pltpu.roll(kva[rows, :].astype(f32), 64, 1).astype(bf16)
 
     lane = iota((128, 128), 1)
     gap = lane - iota((128, 128), 0)
@@ -241,50 +245,68 @@
     first_lane = ones_where((iota((8, 384), 1) & 127) == 0)
     row8 = iota((8, 128), 0)
 
-    def visit(m, own):
-        zq = z + PLANES * m
-        if not own:
-            for copy in query_copies(z, zq):
-                copy.wait_recv()
-
+    def attend_blocks(zq, slot, blocks, masked, gones):
         qa, qb = (qba[zq].astype(f32) * 64.0**-0.5).astype(bf16), qbb[zq]
         zero = jnp.zeros_like(qa)
-        accs, totals = [], []
+        accs, ends_ = [], []
         for h in range(3):
             q = (jnp.where(lane < 64, qa, zero), jnp.where(lane >= 64, qa, zero), qb)[h]
-            gone = jnp.zeros((128, 128), f32)
-            weights = [None] * (PLANES * NX)
-            for b in reversed(range(PLANES * NX)):
-                rows = slice(b * 128, b * 128 + 128)
-                keys = (kva[rows, :], kvr[rows, :], kvb[rows, :128])[h]
+            gone = gones[h]
+            weights = [None] * blocks
+            for b in reversed(range(blocks)):
+                rows = plane_rows(slot, b, 1)
+                keys = (kva, kvr, kvb)[h][rows, :128]
                 scores = dot_tr(q, keys)
                 scores = (scores * 128.0**-0.5 if h == 2 else scores) + off[h : h + 1, rows]
-                valid = gap < ((zq - zp * PLANES) * NX + x - b) * 128
+                valid = gap < (x - b) * 128
                 soft = jnp.maximum(scores, 0.0) + jnp.log(1.0 + jnp.exp(-jnp.abs(scores)))
-                cat = jnp.concatenate(split(jnp.where(valid, soft, 0.0) if own else soft, 2), axis=1)
+                cat = jnp.concatenate(split(jnp.where(valid, soft, 0.0) if masked else soft, 2), axis=1)
                 sums = dot(cat, later_matrix)
                 power = (scores - soft) - (sums[:, :128] + gone)
                 gone = gone + sums[:, 128:]
                 weight = jnp.exp(power)
-                weights[b] = (jnp.where(valid, weight, 0.0) if own else weight).astype(bf16)
-            values = (kvr[...], kva[...], kvb[:, 128:])[h]
+                weights[b] = (jnp.where(valid, weight, 0.0) if masked else weight).astype(bf16)
+            rows = plane_rows(slot, 0, blocks)
+            values = (kvr[rows, :], kva[rows, :], kvb[rows, 128:])[h]
             accs.append(dot(jnp.concatenate(weights, axis=1), values))
-            totals.append(dot_tr(first_lane, jnp.concatenate(split(gone, 3), axis=1)))
-        both = jnp.where(lane < 64, accs[0], accs[1])
-        found = jnp.concatenate([both, accs[2]], axis=1).astype(bf16)
-        sums8 = jnp.where(row8 == 0, totals[0], jnp.where(row8 == 1, totals[1], totals[2]))
-
-        if own:
-            back[z] = found
-            tback[z] = sums8
-        else:
-            ret[zq] = found
-            tot[zq] = sums8
-            for copy in result_copies(zq, z):
-                copy.start()
-
-    visit(0, True)
-    loop(1, groups - zp, lambda m: visit(m, False))
+            ends_.append(gone)
+        return jnp.concatenate([jnp.where(lane < 64, accs[0], accs[1]), accs[2]], axis=1), ends_
+
+    def totals_of(gones):
+        rows3 = [dot_tr(first_lane, jnp.concatenate(split(g, 3), axis=1)) for g in gones]
+        return jnp.where(row8 == 0, rows3[0], jnp.where(row8 == 1, rows3[1], rows3[2]))
+
+    nothing = [jnp.zeros((128, 128), f32)] * 3
+    loop(1, NX, await_keys)
+    swap_sides(here_slot)
+    acc, gones = attend_blocks(z, here_slot, NX, True, nothing)
+    own_acc[...] = acc
+    for h in range(3):
+        own_gone[h] = gones[h]
+    loop(1, NX, await_passed)
+    swap_sides(there_slot)
+
+    @pl.when(zb == 1)
+    def _():
+        acc, gones = attend_blocks(z, 0, NX, False, [own_gone[h] for h in range(3)])
+        own_acc[...] += acc
+        for h in range(3):
+            own_gone[h] = gones[h]
+
+    back[z] = own_acc[...].astype(bf16)
+    tback[z] = totals_of([own_gone[h] for h in range(3)])
+
+    def visit(m):
+        zq = z + PLANES * m
+        for copy in query_copies(z, zq):
+            copy.wait_recv()
+        acc, gones = attend_blocks(zq, 0, PLANES * NX, False, nothing)
+        ret[zq] = acc.astype(bf16)
+        tot[zq] = totals_of(gones)
+        for copy in result_copies(zq, z):
+            copy.start()
+
+    loop(1, groups - zp, visit)
 
     def gather(k, carry):
         acc, gone = carry
@@ -682,6 +704,7 @@
         V((8, 128), f32), V((8, keys), f32), V((nz, 128, 128), bf16), V((nz, 128, 128), bf16),
         V((nz, 128, 256), bf16), V((nz, 128, 256), bf16), V((nz, 8, 128), f32), V((nz, 8, 128), f32),
         dma((3, 2 * NX)), dma((3, 2 * NX)), dma((2, nz)), dma((2, nz)), dma((2, nz)), dma((2, nz)),
+        V((128, 256), f32), V((3, 128, 128), f32),
     ]
     scratch += [
         V((8, 128), f32), V((ntp, 8, 128), f32), dma((ntp,)), dma((ntp,)), V((rows, 256), f32),

time: 116 us -> 115 us (level)
  no operation moved by 1% of the time
where the time goes in v6:
time: 115 us
  Pallas kernels  113 us (98%)
  local copies, waits for them, and re-layouts  1.38 us (1%)
    pallas_call x1, Pallas kernels, body(): pl.pallas_call(functools.partial(layer_kernel, nsp, ntp), out_shape=jax.S...  113 us

profile of v6, /device:TPU:1, one launch (start us, length us, event | category | flops | bytes accessed | tf_op | source)
XLA Modules:
  0.0 114.8 jit_solution(4402139277069175540)
XLA Ops:
  0.0 113.4 %layer.1 = bf16[128,128]{1,0:T(8,128)(2,1)} custom-call(bf16[128,128]{1,0:T(8,128)(2,1)} %qa_ref.1, bf16[128,128]{1,0:T(8,128)(2,1)} %qb_ref.1, bf16[128,128]{1,0:T(8,128)(2,1)} %bitcast.19, bf16[128,256]{1,0:T(8,128)(2,1)} %bitcast.18, f32[2,128]{1,0:T(2,128)} %bitcast.20, f32[1,128]{1,0:T(1,128)} %bitcast.23, bf16[128,128]{1,0:T(8,128)(2,1)} %res_ref.1, ...), custom_call_target="tpu_custom_call" | custom-call | tf_op jit(solution)/shard_map/layer/pallas_call | solution.py:729
  113.4 1.4 %copy.22 = bf16[128,128]{1,0:T(8,128)(2,1)} copy(bf16[128,128]{1,0:T(8,128)(2,1)} %layer.1) | data formatting | bytes 65536
